TPU v7x, 32 devices: a whole 2x2x4 slice. The times are simulated.
32 devices in a mesh: ep: 8 (over z, x), tp: 4 (over y, core).
Axes of the slice: x: 2, y: 2, z: 4, core: 2. Of those that a mesh axis runs over, the one named last changes fastest.
Arguments:
- tokens: bfloat16 [4096, 2048], P(('ep', 'tp')), may hold values from -6 to 6
- routes: int32 [4096, 2], P(('ep', 'tp')), may hold values from 0 to 31, as said below
- gates: float32 [4096, 2], P(('ep', 'tp')), may hold values from 0.1 to 0.6
- w_gate: bfloat16 [32, 2048, 768], P(('ep', 'tp')), may hold values from -0.125 to 0.125
- w_up: bfloat16 [32, 2048, 768], P(('ep', 'tp')), may hold values from -0.125 to 0.125
- w_down: bfloat16 [32, 768, 2048], P(('ep', 'tp')), may hold values from -0.21875 to 0.21875
- moe_out: bfloat16 [4096, 2048], P('ep', 'tp'), may hold values from -16 to 16
- norm_gain: float32 [2048], P('tp'), may hold values from 0.1 to 1.9
- out_grad: bfloat16 [4096, 2048], P('ep', 'tp'), may hold values from -16 to 16
Outputs:
- token_grad: bfloat16 [4096, 2048], P(('ep', 'tp'))
- gates_grad: bfloat16 [4096, 2], P(('ep', 'tp'))
- w_gate_grad: bfloat16 [32, 2048, 768], P(('ep', 'tp'))
- w_up_grad: bfloat16 [32, 2048, 768], P(('ep', 'tp'))
- w_down_grad: bfloat16 [32, 768, 2048], P(('ep', 'tp'))
Inputs may be any that keep to these rules, and one draw needn't show every extreme that they name: `routes`: the two experts of a row differ and lie in one group (expert e is in group e // 8). In the 128 rows of one device the tokens fall into the groups in shares 3/8, 3/8, 1/8, 1/8 of 128, which group takes which share varying. In the rows of one device no expert is named more than 16 times, and one expert is named exactly 16 times in the rows of every device.
All inputs are finite; a program needn't handle non-finite values.
Results may differ from a plain program's by a relative error of at most 0.0071.
Values may be sent and summed in bfloat16 or wider, within the bound.
No kernel may reach another device: no remote copies, remote signals or barrier semaphores. Data moves between devices by JAX's collectives and lax.ppermute only.
A program may use at most 128 MiB of HBM per device.

v0:
```python
import functools

import jax
import jax.numpy as jnp
from jax import lax
from jax.experimental import pallas as pl
from jax.experimental.pallas import tpu as pltpu
from jax.sharding import PartitionSpec as P


epsilon = 1e-06
AXES = ("ep", "tp")
GROUPS = 4
META = 128
GAIN_ROWS = 16
FEATURE_TILES = 4
SMALL_VMEM = 16 * 2**20
BIG_VMEM = 24 * 2**20
SETS = ((1, 2), (3, 0))
TOKEN_SHIFTS = (3, 1, 2)
COT_SHIFTS = (1, 2, 3)
BF = jnp.bfloat16
F32 = jnp.float32


def contract(left, right, left_dim, right_dim):
    return lax.dot_general(
        left, right, (((left_dim,), (right_dim,)), ((), ())), preferred_element_type=F32
    )


def one_hot(column, width):
    lanes = lax.broadcasted_iota(jnp.int32, (column.shape[0], width), 1)
    return jnp.where(column == lanes, 1.0, 0.0).astype(BF)


def strict_lower(rows):
    above = lax.broadcasted_iota(jnp.int32, (rows, rows), 1)
    below = lax.broadcasted_iota(jnp.int32, (rows, rows), 0)
    return jnp.where(above < below, 1.0, 0.0).astype(BF)


def lane_of(column_values, rows):
    lanes = lax.broadcasted_iota(jnp.int32, (rows, META), 1)
    result = jnp.zeros((rows, META), F32)
    for lane, column in enumerate(column_values):
        result = jnp.where(lanes == lane, column, result)
    return result


def place(group_size):
    flat = lax.axis_index("ep") * lax.axis_size("tp") + lax.axis_index("tp")
    return lax.div(flat, group_size), lax.rem(flat, group_size)


def split_kernel(pieces, moe_ref, gain_ref, grad_ref, *out_refs):
    me = lax.axis_index("tp")
    width = moe_ref.shape[1]
    rows = moe_ref.shape[0] // pieces
    gain = gain_ref[...]
    high = gain.astype(BF).astype(F32)
    middle = (gain - high).astype(BF).astype(F32)
    low = gain - high - middle
    line = lax.broadcasted_iota(jnp.int32, (GAIN_ROWS, width), 0)
    parts = jnp.where(line == 0, high, jnp.where(line == 1, middle, 0.0))
    parts = jnp.where(line == 2, low, parts).astype(BF)
    for index in range(pieces):
        first = pl.multiple_of(jnp.bitwise_xor(me, index) * rows, rows)
        out_refs[index][:rows, :width] = grad_ref[pl.ds(first, rows), :]
        out_refs[index][:rows, width:] = moe_ref[pl.ds(first, rows), :]
        out_refs[index][rows:, :width] = parts
        out_refs[index][rows:, width:] = jnp.zeros((GAIN_ROWS, width), BF)


def token_pack_kernel(group_size, share, tok_ref, routes_ref, gates_ref, *refs):
    out_refs, hot_ref, rows_ref = refs[:-2], refs[-2], refs[-1]
    rows, features = tok_ref.shape
    plane, _ = place(group_size)
    rows_ref[...] = jnp.zeros_like(rows_ref)
    rows_ref[0:2, :] = routes_ref[...].astype(F32)
    rows_ref[2:4, :] = gates_ref[...]
    unit_row = lax.broadcasted_iota(jnp.int32, (rows, rows), 0)
    unit_col = lax.broadcasted_iota(jnp.int32, (rows, rows), 1)
    unit = jnp.where(unit_row == unit_col, 1.0, 0.0).astype(BF)
    columns = contract(unit, rows_ref[...].astype(BF), 1, 1)
    first = columns[:, 0:1].astype(jnp.int32)
    second = columns[:, 1:2].astype(jnp.int32)
    group = lax.div(first, group_size)
    shift = lax.rem(group - plane + GROUPS, GROUPS)
    member = one_hot(shift, META)
    before = contract(strict_lower(rows), member, 1, 0)
    rank = jnp.sum(before * member.astype(F32), axis=1, keepdims=True).astype(jnp.int32)
    hot = one_hot(shift * share + rank, GROUPS * share)
    hot_ref[...] = hot
    base = group * group_size
    meta = lane_of(
        (
            (first - base + 1).astype(F32),
            (second - base + 1).astype(F32),
            columns[:, 2:3],
            columns[:, 3:4],
        ),
        rows,
    ).astype(BF)
    packed = contract(hot, tok_ref[...], 0, 0).astype(BF)
    packed_meta = contract(hot, meta, 0, 0).astype(BF)
    for index in range(GROUPS):
        out_refs[index][:, :features] = packed[index * share : (index + 1) * share]
        out_refs[index][:, features:] = packed_meta[index * share : (index + 1) * share]


def cot_pack_kernel(pieces, share, *refs):
    piece_refs, hot_ref = refs[:pieces], refs[pieces]
    out_refs, full_ref = refs[pieces + 1 : -1], refs[-1]
    me = lax.axis_index("tp")
    rows = hot_ref.shape[0]
    width = piece_refs[0].shape[1] // 2
    features = width * pieces

    def read(ref):
        gain = jnp.sum(ref[rows:, :width].astype(F32), axis=0, keepdims=True)
        return ref[:rows, width:].astype(F32), gain * ref[:rows, :width].astype(F32)

    square_sum = 0.0
    cross_sum = 0.0
    for ref in piece_refs:
        saved, scaled = read(ref)
        square_sum += jnp.sum(saved * saved, axis=1, keepdims=True)
        cross_sum += jnp.sum(saved * scaled, axis=1, keepdims=True)
    inv_rms = lax.rsqrt(square_sum / features + epsilon)
    factor = inv_rms * inv_rms * inv_rms * cross_sum / features
    for index, ref in enumerate(piece_refs):
        saved, scaled = read(ref)
        column = pl.multiple_of(jnp.bitwise_xor(me, index) * width, width)
        full_ref[:, pl.ds(column, width)] = (inv_rms * scaled - saved * factor).astype(BF)
    packed = contract(hot_ref[...], full_ref[...], 0, 0).astype(BF)
    for index in range(GROUPS):
        out_refs[index][...] = packed[index * share : (index + 1) * share]


def token_route_kernel(group_size, capacity, *refs):
    shifts = len(refs) - group_size - 3
    msg_refs, out_refs = refs[:shifts], refs[shifts : shifts + group_size]
    hot0_ref, hot1_ref, full_ref = refs[-3:]
    share, width = msg_refs[0].shape
    features = width - META
    slots = shifts * capacity
    _, mine = place(group_size)
    lower = strict_lower(share)
    gates = []
    for index, ref in enumerate(msg_refs):
        row = slice(index * share, (index + 1) * share)
        full_ref[row, :] = ref[:, :features]
        meta = ref[:, features:].astype(F32)
        gates.append((meta[:, 2:3], meta[:, 3:4]))
        experts = [meta[:, k : k + 1].astype(jnp.int32) - 1 for k in range(2)]
        members = [one_hot(e, META) for e in experts]
        before = contract(lower, members[0] + members[1], 1, 0)
        for expert, member, hot_ref in zip(experts, members, (hot0_ref, hot1_ref)):
            rank = jnp.sum(before * member.astype(F32), axis=1, keepdims=True)
            slot = jnp.bitwise_xor(expert, mine) * slots + index * capacity
            slot = jnp.where(expert < 0, -1, slot + rank.astype(jnp.int32))
            hot_ref[row, :] = one_hot(slot, group_size * slots)
    hot0, hot1 = hot0_ref[...], hot1_ref[...]
    total = shifts * share
    gate0 = lane_of((jnp.concatenate([g[0] for g in gates], axis=0),), total).astype(BF)
    gate1 = lane_of((jnp.concatenate([g[1] for g in gates], axis=0),), total).astype(BF)
    packed_gate = contract(hot0, gate0, 0, 0) + contract(hot1, gate1, 0, 0)
    packed = contract(hot0 + hot1, full_ref[...], 0, 0)
    for index in range(group_size):
        row = slice(index * slots, (index + 1) * slots)
        out_refs[index][:, :features] = packed[row].astype(BF)
        out_refs[index][:, features:] = packed_gate[row].astype(BF)


def cot_route_kernel(group_size, *refs):
    shifts = len(refs) - group_size - 3
    msg_refs, hot0_ref, hot1_ref = refs[:shifts], refs[shifts], refs[shifts + 1]
    out_refs, full_ref = refs[shifts + 2 : -1], refs[-1]
    share = msg_refs[0].shape[0]
    slots = hot0_ref.shape[1] // group_size
    for index, ref in enumerate(msg_refs):
        full_ref[index * share : (index + 1) * share, :] = ref[...]
    packed = contract(hot0_ref[...] + hot1_ref[...], full_ref[...], 0, 0)
    for index in range(group_size):
        out_refs[index][...] = packed[index * slots : (index + 1) * slots].astype(BF)


def combine_kernel(group_size, shifts, *refs):
    piece_refs, hot0_ref, hot1_ref = refs[:group_size], refs[group_size], refs[group_size + 1]
    out_refs = refs[group_size + 2 :]
    features = piece_refs[0].shape[1] - META
    share = hot0_ref.shape[0] // shifts
    rows = jnp.concatenate([ref[...].astype(F32) for ref in piece_refs], axis=0).astype(BF)
    hot0, hot1 = hot0_ref[...], hot1_ref[...]
    summed = contract(hot0 + hot1, rows[:, :features], 1, 0).astype(BF)
    grad0 = contract(hot0, rows[:, features:], 1, 0)[:, 0:1]
    grad1 = contract(hot1, rows[:, features:], 1, 0)[:, 0:1]
    meta = lane_of((grad0, grad1), shifts * share).astype(BF)
    for index in range(shifts):
        row = slice(index * share, (index + 1) * share)
        out_refs[index][:, :features] = summed[row]
        out_refs[index][:, features:] = meta[row]


def finish_kernel(hot_ref, *refs):
    msg_refs, tok_ref, gates_ref = refs[:GROUPS], refs[-2], refs[-1]
    features = tok_ref.shape[1]
    rows = jnp.concatenate([ref[...] for ref in msg_refs], axis=0)
    hot = hot_ref[...]
    tok_ref[...] = contract(hot, rows[:, :features], 1, 0).astype(BF)
    grads = contract(rows[:, features:].astype(F32).T.astype(BF), hot, 1, 1)
    gates_ref[...] = grads[0:2].astype(BF)


def forward_kernel(*refs):
    count = len(refs) - 6
    piece_refs, (gate_ref, up_ref) = refs[:count], refs[count : count + 2]
    rows_ref, meta_ref, pre_gate_ref, pre_up_ref = refs[count + 2 :]
    features = rows_ref.shape[1]
    first = 0
    for ref in piece_refs:
        last = first + ref.shape[0]
        rows_ref[first:last, :] = ref[:, :features]
        meta_ref[first:last, :] = ref[:, features:]
        first = last
    rows = rows_ref[...]
    pre_gate_ref[...] = contract(rows, gate_ref[0], 1, 0)
    pre_up_ref[...] = contract(rows, up_ref[0], 1, 0)


def backward_kernel(group_size, first, *refs):
    piece_refs = refs[:group_size]
    meta_ref, pre_gate_ref, pre_up_ref, gate_ref, up_ref, down_ref = refs[
        group_size : group_size + 6
    ]
    out_refs = refs[group_size + 6 : 2 * group_size + 6]
    d_gate_ref, d_up_ref, hidden_ref, scaled_ref, cot_ref = refs[2 * group_size + 6 :]
    slots, features = piece_refs[0].shape
    rows = cot_ref.shape[0]
    held = slice(first, first + rows)
    for index, ref in enumerate(piece_refs):
        cot_ref[index * slots : (index + 1) * slots, :] = ref[...]
    weight = meta_ref[held, 0:1].astype(F32)
    hid_grad = contract(cot_ref[...], down_ref[0], 1, 1)
    pre_gate, pre_up = pre_gate_ref[held, :], pre_up_ref[held, :]
    sigmoid_gate = jax.nn.sigmoid(pre_gate)
    activated = pre_gate * sigmoid_gate
    hidden = activated * pre_up
    grad = lane_of((jnp.sum(hidden * hid_grad, axis=1, keepdims=True),), rows).astype(BF)
    d_hidden = weight * hid_grad
    d_gate_ref[...] = (
        d_hidden * pre_up * sigmoid_gate * (1.0 + pre_gate * (1.0 - sigmoid_gate))
    ).astype(BF)
    d_up_ref[...] = (d_hidden * activated).astype(BF)
    hidden_ref[...] = hidden.astype(BF)
    tile = features // FEATURE_TILES
    for start in range(0, features, tile):
        column = slice(start, start + tile)
        back = contract(d_gate_ref[...], gate_ref[0, column, :], 1, 1)
        back = (back + contract(d_up_ref[...], up_ref[0, column, :], 1, 1)).astype(BF)
        for index, ref in enumerate(out_refs):
            ref[:, column] = back[index * slots : (index + 1) * slots]
    for index, ref in enumerate(out_refs):
        ref[:, features:] = grad[index * slots : (index + 1) * slots]
    scaled_ref[...] = (weight * cot_ref[...].astype(F32)).astype(BF)


def weight_kernel(sets, rows_ref, *refs):
    d_gate, d_up, hidden, scaled = (refs[k * sets : (k + 1) * sets] for k in range(4))
    grad_gate_ref, grad_up_ref, grad_down_ref, both_ref, turned_ref = refs[4 * sets :]
    hidden_width = hidden[0].shape[1]

    @pl.when(pl.program_id(0) == 0)
    def _():
        first = 0
        for gate, up, hid in zip(d_gate, d_up, hidden):
            last = first + gate.shape[0]
            both_ref[first:last, :hidden_width] = gate[...]
            both_ref[first:last, hidden_width:] = up[...]
            turned_ref[:, first:last] = hid[...].T
            first = last

    both = contract(rows_ref[...], both_ref[...], 0, 0)
    grad_gate_ref[0] = both[:, :hidden_width].astype(BF)
    grad_up_ref[0] = both[:, hidden_width:].astype(BF)
    cots = jnp.concatenate([ref[...] for ref in scaled], axis=0)
    grad_down_ref[0] = contract(turned_ref[...], cots, 1, 0).astype(BF)


def forward_call(pieces, w_gate, w_up):
    features, hidden = w_gate.shape[1:]
    rows = sum(p.shape[0] for p in pieces)
    return call(
        forward_kernel,
        [(rows, features), (rows, META), (rows, hidden, F32), (rows, hidden, F32)],
        [*pieces, w_gate, w_up],
        flops=4 * rows * features * hidden,
        limit=BIG_VMEM,
    )


def backward_call(first, pieces, *held):
    features, hidden = held[3].shape[1:]
    slots = pieces[0].shape[0]
    rows = slots * len(pieces)
    result = call(
        functools.partial(backward_kernel, len(pieces), first),
        [(slots, features + META)] * len(pieces) + [(rows, hidden)] * 3 + [(rows, features)],
        [*pieces, *held],
        scratch=[((rows, features), BF)],
        flops=6 * rows * features * hidden,
        limit=BIG_VMEM,
    )
    return result[: len(pieces)], result[len(pieces) :]


def weight_call(rows, kept):
    d_gate, d_up, hidden, scaled = ([k[i] for k in kept] for i in range(4))
    total, features = rows.shape
    width = hidden[0].shape[1]
    tile = features // FEATURE_TILES
    whole = lambda a: pl.BlockSpec(a.shape, lambda d: (0, 0))
    return pl.pallas_call(
        functools.partial(weight_kernel, len(kept)),
        grid=(FEATURE_TILES,),
        out_shape=[
            jax.ShapeDtypeStruct((1, features, width), BF),
            jax.ShapeDtypeStruct((1, features, width), BF),
            jax.ShapeDtypeStruct((1, width, features), BF),
        ],
        in_specs=[pl.BlockSpec((total, tile), lambda d: (0, d))]
        + [whole(a) for a in (*d_gate, *d_up, *hidden)]
        + [pl.BlockSpec((a.shape[0], tile), lambda d: (0, d)) for a in scaled],
        out_specs=[
            pl.BlockSpec((1, tile, width), lambda d: (0, d, 0)),
            pl.BlockSpec((1, tile, width), lambda d: (0, d, 0)),
            pl.BlockSpec((1, width, tile), lambda d: (0, 0, d)),
        ],
        scratch_shapes=[pltpu.VMEM((total, 2 * width), BF), pltpu.VMEM((width, total), BF)],
        compiler_params=pltpu.CompilerParams(vmem_limit_bytes=BIG_VMEM),
        cost_estimate=pl.CostEstimate(
            flops=6 * total * features * width,
            bytes_accessed=6 * features * width + 4 * total * features + 6 * total * width,
            transcendentals=0,
        ),
    )(rows, *d_gate, *d_up, *hidden, *scaled)


def call(kernel, outs, args, scratch=(), flops=0, limit=SMALL_VMEM):
    outs = [jax.ShapeDtypeStruct(o[:2], o[2] if len(o) > 2 else BF) for o in outs]
    size = sum(a.size * a.dtype.itemsize for a in (*args, *outs))
    return pl.pallas_call(
        kernel,
        out_shape=outs,
        in_specs=[pl.BlockSpec(memory_space=pltpu.VMEM)] * len(args),
        out_specs=[pl.BlockSpec(memory_space=pltpu.VMEM)] * len(outs),
        scratch_shapes=[pltpu.VMEM(shape, dtype) for shape, dtype in scratch],
        compiler_params=pltpu.CompilerParams(vmem_limit_bytes=limit),
        cost_estimate=pl.CostEstimate(flops=flops, bytes_accessed=size, transcendentals=0),
    )(*args)


def local(tokens, routes, gates, w_gate, w_up, w_down, moe_out, norm_gain, out_grad):
    devices = lax.axis_size(AXES)
    pieces = lax.axis_size("tp")
    group_size = devices // GROUPS
    tok_rows, features = tokens.shape
    capacity = 4 * tok_rows // devices
    share = 3 * tok_rows // 8
    wide = features + META

    def over_tp(array, bits):
        pairs = [(d, d ^ bits) for d in range(pieces)]
        return lax.ppermute(array, "tp", pairs)

    def over_plane(array, bits):
        pairs = [
            (d, d // group_size * group_size + (d % group_size ^ bits)) for d in range(devices)
        ]
        return lax.ppermute(array, AXES, pairs)

    def over_z(array, shift):
        pairs = [(d, (d + shift * group_size) % devices) for d in range(devices)]
        return lax.ppermute(array, AXES, pairs)

    part = [(tok_rows + GAIN_ROWS, 2 * moe_out.shape[1])] * pieces
    *tok_msgs, hot = call(
        functools.partial(token_pack_kernel, group_size, share),
        [(share, wide)] * GROUPS + [(tok_rows, GROUPS * share)],
        (tokens, routes.T, gates.T),
        scratch=[((8, tok_rows), F32)],
        flops=2 * tok_rows * GROUPS * share * wide,
    )
    tok_at = {0: tok_msgs[0]}
    for s in TOKEN_SHIFTS:
        tok_at[s] = over_z(tok_msgs[s], s)
    split = call(
        functools.partial(split_kernel, pieces), part, (moe_out, norm_gain[None, :], out_grad)
    )
    split = [split[0]] + [over_tp(split[m], m) for m in range(1, pieces)]
    cot_msgs = call(
        functools.partial(cot_pack_kernel, pieces, share),
        [(share, features)] * GROUPS,
        (*split, hot),
        scratch=[((tok_rows, features), BF)],
        flops=2 * tok_rows * GROUPS * share * features,
    )
    cot_at = {0: cot_msgs[0]}
    for s in COT_SHIFTS:
        cot_at[s] = over_z(cot_msgs[s], s)

    hots, tok_in, cot_in = [], [], []
    for group in SETS:
        count = len(group)
        slots = count * capacity
        *out, hot0, hot1 = call(
            functools.partial(token_route_kernel, group_size, capacity),
            [(slots, wide)] * group_size + [(count * share, group_size * slots)] * 2,
            [tok_at[s] for s in group],
            scratch=[((count * share, features), BF)],
            flops=2 * count * share * group_size * slots * wide,
        )
        hots.append((hot0, hot1))
        tok_in.append([out[0]] + [over_plane(out[m], m) for m in range(1, group_size)])
    for group, (hot0, hot1) in zip(SETS, hots):
        count = len(group)
        slots = count * capacity
        out = call(
            functools.partial(cot_route_kernel, group_size),
            [(slots, features)] * group_size,
            [cot_at[s] for s in group] + [hot0, hot1],
            scratch=[((count * share, features), BF)],
            flops=2 * count * share * group_size * slots * features,
        )
        cot_in.append([out[0]] + [over_plane(out[m], m) for m in range(1, group_size)])

    row_block, meta, pre_gate, pre_up = forward_call([p for t in tok_in for p in t], w_gate, w_up)
    backs, kept, first = [], [], 0
    for cots in cot_in:
        back, keep = backward_call(first, cots, meta, pre_gate, pre_up, w_gate, w_up, w_down)
        first += cots[0].shape[0] * group_size
        backs.append([back[0]] + [over_plane(back[m], m) for m in range(1, group_size)])
        kept.append(keep)
    grad_gate, grad_up, grad_down = weight_call(row_block, kept)

    home = {}
    for group, back, (hot0, hot1) in zip(SETS, backs, hots):
        count = len(group)
        out = call(
            functools.partial(combine_kernel, group_size, count),
            [(share, wide)] * count,
            [*back, hot0, hot1],
            flops=2 * hot0.size * wide,
        )
        for s, array in zip(group, out):
            home[s] = over_z(array, -s) if s else array
    token_grad, gates_grad = call(
        finish_kernel,
        [(tok_rows, features), (routes.shape[1], tok_rows)],
        [hot] + [home[s] for s in range(GROUPS)],
        flops=2 * hot.size * wide,
    )
    return (token_grad, gates_grad.T, grad_gate, grad_up, grad_down)


def solution(mesh):
    in_specs = (
        P(AXES, None),
        P(AXES, None),
        P(AXES, None),
        P(AXES, None, None),
        P(AXES, None, None),
        P(AXES, None, None),
        P("ep", "tp"),
        P("tp"),
        P("ep", "tp"),
    )
    out_specs = (
        P(AXES, None),
        P(AXES, None),
        P(AXES, None, None),
        P(AXES, None, None),
        P(AXES, None, None),
    )

    return jax.shard_map(local, mesh=mesh, in_specs=in_specs, out_specs=out_specs, check_vma=False)
```

profile of v0, /device:TPU:0, one launch (start us, length us, event | category | flops | bytes accessed | tf_op | source)
XLA Modules:
  0.0 144.7 jit_solution(15041266790822234687)
XLA Ops:
  4.1 3.1 %collective-permute-start.12 = (bf16[48,2176]{1,0:T(8,128)(2,1)S(1)}, bf16[48,2176]{1,0:T(8,128)(2,1)S(1)}, u32[]{:S(2)}, u32[]{:S(2)}) collective-permute-start(bf16[48,2176]{1,0:T(8,128)(2,1)S(1)} %get-tuple-element.110), channel_id=1, source_target_pairs={{0,8},{1,9},{2,10},{3,11},{4,12},{5,13},{6,14},{7,15},{8,16},{9,17... | collective-permute-start | bytes 626696 | tf_op jit(solution)/shard_map/ppermute | solution.py:385
  7.2 2.6 %collective-permute-start.13 = (bf16[48,2176]{1,0:T(8,128)(2,1)S(1)}, bf16[48,2176]{1,0:T(8,128)(2,1)S(1)}, u32[]{:S(2)}, u32[]{:S(2)}) collective-permute-start(bf16[48,2176]{1,0:T(8,128)(2,1)S(1)} %get-tuple-element.111), channel_id=1, source_target_pairs={{0,16},{1,17},{2,18},{3,19},{4,20},{5,21},{6,22},{7,23},{8,24},{9,... | collective-permute-start | bytes 626696 | tf_op jit(solution)/shard_map/ppermute | solution.py:385
  16.5 7.0 %collective-permute-done.13.refs_1_ = bf16[48,2176]{1,0:T(8,128)(2,1)S(1)} collective-permute-done((bf16[48,2176]{1,0:T(8,128)(2,1)S(1)}, bf16[48,2176]{1,0:T(8,128)(2,1)S(1)}, u32[]{:S(2)}, u32[]{:S(2)}) %collective-permute-start.13) | collective-permute-done | bytes 208928 | tf_op jit(solution)/shard_map/ppermute | solution.py:385
  24.5 2.6 %collective-permute-done.4.refs_0_ = bf16[48,2176]{1,0:T(8,128)(2,1)S(1)} collective-permute-done((bf16[48,2176]{1,0:T(8,128)(2,1)S(1)}, bf16[48,2176]{1,0:T(8,128)(2,1)S(1)}, u32[]{:S(2)}, u32[]{:S(2)}) %collective-permute-start.4) | collective-permute-done | bytes 208928 | tf_op jit(solution)/shard_map/ppermute | solution.py:385
  30.6 2.4 %collective-permute-start.19 = (bf16[32,2176]{1,0:T(8,128)(2,1)S(1)}, bf16[32,2176]{1,0:T(8,128)(2,1)S(1)}, u32[]{:S(2)}, u32[]{:S(2)}) collective-permute-start(bf16[32,2176]{1,0:T(8,128)(2,1)S(1)} %get-tuple-element.118), channel_id=1, source_target_pairs={{0,6},{1,7},{2,4},{3,5},{4,2},{5,3},{6,0},{7,1},{8,14},{9,15},{10,... | collective-permute-start | bytes 417800 | tf_op jit(solution)/shard_map/ppermute | solution.py:381
  34.9 2.5 %collective-permute-start.35 = (bf16[48,2048]{1,0:T(8,128)(2,1)S(1)}, bf16[48,2048]{1,0:T(8,128)(2,1)S(1)}, u32[]{:S(2)}, u32[]{:S(2)}) collective-permute-start(bf16[48,2048]{1,0:T(8,128)(2,1)S(1)} %get-tuple-element.140), channel_id=1, source_target_pairs={{0,8},{1,9},{2,10},{3,11},{4,12},{5,13},{6,14},{7,15},{8,16},{9,17... | collective-permute-start | bytes 589832 | tf_op jit(solution)/shard_map/ppermute | solution.py:385
  37.4 2.8 %collective-permute-start.21 = (bf16[32,2176]{1,0:T(8,128)(2,1)S(1)}, bf16[32,2176]{1,0:T(8,128)(2,1)S(1)}, u32[]{:S(2)}, u32[]{:S(2)}) collective-permute-start(bf16[32,2176]{1,0:T(8,128)(2,1)S(1)} %get-tuple-element.121), channel_id=1, source_target_pairs={{0,1},{1,0},{2,3},{3,2},{4,5},{5,4},{6,7},{7,6},{8,9},{9,8},{10,11... | collective-permute-start | bytes 417800 | tf_op jit(solution)/shard_map/ppermute | solution.py:381
  41.6 2.6 %collective-permute-done.20.refs_7_ = bf16[32,2176]{1,0:T(8,128)(2,1)S(1)} collective-permute-done((bf16[32,2176]{1,0:T(8,128)(2,1)S(1)}, bf16[32,2176]{1,0:T(8,128)(2,1)S(1)}, u32[]{:S(2)}, u32[]{:S(2)}) %collective-permute-start.20) | collective-permute-done | bytes 139296 | tf_op jit(solution)/shard_map/ppermute | solution.py:381
  44.2 3.9 %collective-permute-start.36 = (bf16[48,2048]{1,0:T(8,128)(2,1)S(1)}, bf16[48,2048]{1,0:T(8,128)(2,1)S(1)}, u32[]{:S(2)}, u32[]{:S(2)}) collective-permute-start(bf16[48,2048]{1,0:T(8,128)(2,1)S(1)} %get-tuple-element.141), channel_id=1, source_target_pairs={{0,16},{1,17},{2,18},{3,19},{4,20},{5,21},{6,22},{7,23},{8,24},{9,... | collective-permute-start | bytes 589832 | tf_op jit(solution)/shard_map/ppermute | solution.py:385
  52.4 5.2 %collective-permute-done.36.refs_1_ = bf16[48,2048]{1,0:T(8,128)(2,1)S(1)} collective-permute-done((bf16[48,2048]{1,0:T(8,128)(2,1)S(1)}, bf16[48,2048]{1,0:T(8,128)(2,1)S(1)}, u32[]{:S(2)}, u32[]{:S(2)}) %collective-permute-start.36) | collective-permute-done | bytes 196640 | tf_op jit(solution)/shard_map/ppermute | solution.py:385
  70.9 1.9 %copy-done.1 = bf16[1,2048,768]{2,1,0:T(8,128)(2,1)S(1)} copy-done((bf16[1,2048,768]{2,1,0:T(8,128)(2,1)S(1)}, bf16[1,2048,768]{2,1,0:T(8,128)(2,1)}, u32[]{:S(2)}) %copy-start.1) | copy-done | bytes 3145752
  72.8 3.4 %shard_map.134 = (bf16[512,2048]{1,0:T(8,128)(2,1)S(1)}, bf16[512,128]{1,0:T(8,128)(2,1)S(1)}, f32[512,768]{1,0:T(8,128)S(1)}, f32[512,768]{1,0:T(8,128)S(1)}) custom-call(bf16[32,2176]{1,0:T(8,128)(2,1)S(1)} %get-tuple-element.112.refs_0_, bf16[32,2176]{1,0:T(8,128)(2,1)S(1)} %collective-permute-done.14.refs_1_, ...), custom_call_target="tpu_custom_call" | custom-call | flops 3221225472 | bytes 13893632 | tf_op jit(solution)/shard_map/pallas_call | solution.py:353
  81.5 3.1 %shard_map.138 = (bf16[32,2176]{1,0:T(8,128)(2,1)S(1)}, bf16[32,2176]{1,0:T(8,128)(2,1)S(1)}, bf16[32,2176]{1,0:T(8,128)(2,1)S(1)}, bf16[32,2176]{1,0:T(8,128)(2...) custom-call(bf16[32,2048]{1,0:T(8,128)(2,1)S(1)} %get-tuple-element., ...), custom_call_target="tpu_custom_call" | custom-call | flops 2415919104 | bytes 17104896 | tf_op jit(solution)/shard_map/pallas_call | solution.py:353
  86.0 3.5 %collective-permute-done.10.refs_6_ = bf16[32,2048]{1,0:T(8,128)(2,1)S(1)} collective-permute-done((bf16[32,2048]{1,0:T(8,128)(2,1)S(1)}, bf16[32,2048]{1,0:T(8,128)(2,1)S(1)}, u32[]{:S(2)}, u32[]{:S(2)}) %collective-permute-start.10) | collective-permute-done | bytes 131104 | tf_op jit(solution)/shard_map/ppermute | solution.py:381
  91.3 3.1 %shard_map.135 = (bf16[32,2176]{1,0:T(8,128)(2,1)S(1)}, bf16[32,2176]{1,0:T(8,128)(2,1)S(1)}, bf16[32,2176]{1,0:T(8,128)(2,1)S(1)}, bf16[32,2176]{1,0:T(8,128)(2...) custom-call(bf16[32,2048]{1,0:T(8,128)(2,1)S(1)} %get-tuple-element., ...), custom_call_target="tpu_custom_call" | custom-call | flops 2415919104 | bytes 17104896 | tf_op jit(solution)/shard_map/pallas_call | solution.py:353
  105.1 1.9 %collective-permute-start.48 = (bf16[32,2176]{1,0:T(8,128)(2,1)S(1)}, bf16[32,2176]{1,0:T(8,128)(2,1)S(1)}, u32[]{:S(2)}, u32[]{:S(2)}) collective-permute-start(bf16[32,2176]{1,0:T(8,128)(2,1)S(1)} %get-tuple-element.157), channel_id=1, source_target_pairs={{0,5},{1,4},{2,7},{3,6},{4,1},{5,0},{6,3},{7,2},{8,13},{9,12},{10,... | collective-permute-start | bytes 417800 | tf_op jit(solution)/shard_map/ppermute | solution.py:381
  107.0 2.5 %collective-permute-done.33.refs_6_ = bf16[32,2176]{1,0:T(8,128)(2,1)S(1)} collective-permute-done((bf16[32,2176]{1,0:T(8,128)(2,1)S(1)}, bf16[32,2176]{1,0:T(8,128)(2,1)S(1)}, u32[]{:S(2)}, u32[]{:S(2)}) %collective-permute-start.33) | collective-permute-done | bytes 139296 | tf_op jit(solution)/shard_map/ppermute | solution.py:381
  111.8 1.8 %collective-permute-start.50 = (bf16[32,2176]{1,0:T(8,128)(2,1)S(1)}, bf16[32,2176]{1,0:T(8,128)(2,1)S(1)}, u32[]{:S(2)}, u32[]{:S(2)}) collective-permute-start(bf16[32,2176]{1,0:T(8,128)(2,1)S(1)} %get-tuple-element.159), channel_id=1, source_target_pairs={{0,7},{1,6},{2,5},{3,4},{4,3},{5,2},{6,1},{7,0},{8,15},{9,14},{10,... | collective-permute-start | bytes 417800 | tf_op jit(solution)/shard_map/ppermute | solution.py:381
  114.2 3.6 %collective-permute-start.53 = (bf16[48,2176]{1,0:T(8,128)(2,1)S(1)}, bf16[48,2176]{1,0:T(8,128)(2,1)S(1)}, u32[]{:S(2)}, u32[]{:S(2)}) collective-permute-start(bf16[48,2176]{1,0:T(8,128)(2,1)S(1)} %get-tuple-element.162), channel_id=1, source_target_pairs={{0,8},{1,9},{2,10},{3,11},{4,12},{5,13},{6,14},{7,15},{8,16},{9,17... | collective-permute-start | bytes 626696 | tf_op jit(solution)/shard_map/ppermute | solution.py:385
  117.9 3.6 %collective-permute-done.49.refs_6_ = bf16[32,2176]{1,0:T(8,128)(2,1)S(1)} collective-permute-done((bf16[32,2176]{1,0:T(8,128)(2,1)S(1)}, bf16[32,2176]{1,0:T(8,128)(2,1)S(1)}, u32[]{:S(2)}, u32[]{:S(2)}) %collective-permute-start.49) | collective-permute-done | bytes 139296 | tf_op jit(solution)/shard_map/ppermute | solution.py:381
  121.4 2.2 %collective-permute-done.50.refs_7_ = bf16[32,2176]{1,0:T(8,128)(2,1)S(1)} collective-permute-done((bf16[32,2176]{1,0:T(8,128)(2,1)S(1)}, bf16[32,2176]{1,0:T(8,128)(2,1)S(1)}, u32[]{:S(2)}, u32[]{:S(2)}) %collective-permute-start.50) | collective-permute-done | bytes 139296 | tf_op jit(solution)/shard_map/ppermute | solution.py:381
  124.1 6.6 %collective-permute-start.51 = (bf16[48,2176]{1,0:T(8,128)(2,1)S(1)}, bf16[48,2176]{1,0:T(8,128)(2,1)S(1)}, u32[]{:S(2)}, u32[]{:S(2)}) collective-permute-start(bf16[48,2176]{1,0:T(8,128)(2,1)S(1)} %get-tuple-element.160), channel_id=1, source_target_pairs={{0,24},{1,25},{2,26},{3,27},{4,28},{5,29},{6,30},{7,31},{8,0},{9,1... | collective-permute-start | bytes 626696 | tf_op jit(solution)/shard_map/ppermute | solution.py:385
  130.7 7.4 %shard_map.141 = (bf16[1,2048,768]{2,1,0:T(8,128)(2,1)}, bf16[1,2048,768]{2,1,0:T(8,128)(2,1)}, bf16[1,768,2048]{2,1,0:T(8,128)(2,1)}) custom-call(bf16[512,2048]{1,0:T(8,128)(2,1)S(1)} %get-tuple-element.165.rows_ref, bf16[256,768]{1,0:T(8,128)(2,1)S(1)} %get-tuple-element.166.refs_0_, bf16[256,768]{1,0:T(8,128)(2,1)S(1)} %get-tuple-element.167.refs_1_, ...), custom_call_target="tpu_custom_call" | custom-call | flops 4831838208 | bytes 15990784 | tf_op jit(solution)/shard_map/pallas_call | solution.py:324
  138.1 5.4 %collective-permute-done.52.refs_2_ = bf16[48,2176]{1,0:T(8,128)(2,1)S(1)} collective-permute-done((bf16[48,2176]{1,0:T(8,128)(2,1)S(1)}, bf16[48,2176]{1,0:T(8,128)(2,1)S(1)}, u32[]{:S(2)}, u32[]{:S(2)}) %collective-permute-start.52) | collective-permute-done | bytes 208928 | tf_op jit(solution)/shard_map/ppermute | solution.py:385
  (118 shorter events, 58.9 us)
Async XLA Ops:
  4.1 11.2 %collective-permute-start.12 = (bf16[48,2176]{1,0:T(8,128)(2,1)S(1)}, bf16[48,2176]{1,0:T(8,128)(2,1)S(1)}, u32[]{:S(2)}, u32[]{:S(2)}) collective-permute-start(bf16[48,2176]{1,0:T(8,128)(2,1)S(1)} %get-tuple-element.110), channel_id=1, source_target_pairs={{0,8},{1,9},{2,10},{3,11},{4,12},{5,13},{6,14},{7,15},{8,16},{9,17... | collective-permute-start | bytes 626696 | tf_op jit(solution)/shard_map/ppermute | solution.py:385
  7.2 16.3 %collective-permute-start.13 = (bf16[48,2176]{1,0:T(8,128)(2,1)S(1)}, bf16[48,2176]{1,0:T(8,128)(2,1)S(1)}, u32[]{:S(2)}, u32[]{:S(2)}) collective-permute-start(bf16[48,2176]{1,0:T(8,128)(2,1)S(1)} %get-tuple-element.111), channel_id=1, source_target_pairs={{0,16},{1,17},{2,18},{3,19},{4,20},{5,21},{6,22},{7,23},{8,24},{9,... | collective-permute-start | bytes 626696 | tf_op jit(solution)/shard_map/ppermute | solution.py:385
  12.7 15.9 %collective-permute-start = (bf16[144,1024]{1,0:T(8,128)(2,1)S(1)}, bf16[144,1024]{1,0:T(8,128)(2,1)S(1)}, u32[]{:S(2)}, u32[]{:S(2)}) collective-permute-start(bf16[144,1024]{1,0:T(8,128)(2,1)S(1)} %get-tuple-element.93), channel_id=1, source_target_pairs={{0,1},{1,0},{2,3},{3,2},{4,5},{5,4},{6,7},{7,6},{8,9},{9,8},{10,11... | collective-permute-start | bytes 884744 | tf_op jit(solution)/shard_map/ppermute | solution.py:375
  12.8 15.9 %collective-permute-start.1 = (bf16[144,1024]{1,0:T(8,128)(2,1)S(1)}, bf16[144,1024]{1,0:T(8,128)(2,1)S(1)}, u32[]{:S(2)}, u32[]{:S(2)}) collective-permute-start(bf16[144,1024]{1,0:T(8,128)(2,1)S(1)} %get-tuple-element.94), channel_id=1, source_target_pairs={{0,2},{1,3},{2,0},{3,1},{4,6},{5,7},{6,4},{7,5},{8,10},{9,11},{10,... | collective-permute-start | bytes 884744 | tf_op jit(solution)/shard_map/ppermute | solution.py:375
  14.3 15.8 %collective-permute-start.2 = (bf16[144,1024]{1,0:T(8,128)(2,1)S(1)}, bf16[144,1024]{1,0:T(8,128)(2,1)S(1)}, u32[]{:S(2)}, u32[]{:S(2)}) collective-permute-start(bf16[144,1024]{1,0:T(8,128)(2,1)S(1)} %get-tuple-element.95), channel_id=1, source_target_pairs={{0,3},{1,2},{2,1},{3,0},{4,7},{5,6},{6,5},{7,4},{8,11},{9,10},{10,... | collective-permute-start | bytes 884744 | tf_op jit(solution)/shard_map/ppermute | solution.py:375
  15.4 11.7 %collective-permute-start.4 = (bf16[48,2176]{1,0:T(8,128)(2,1)S(1)}, bf16[48,2176]{1,0:T(8,128)(2,1)S(1)}, u32[]{:S(2)}, u32[]{:S(2)}) collective-permute-start(bf16[48,2176]{1,0:T(8,128)(2,1)S(1)} %get-tuple-element.98), channel_id=1, source_target_pairs={{0,24},{1,25},{2,26},{3,27},{4,28},{5,29},{6,30},{7,31},{8,0},{9,1... | collective-permute-start | bytes 626696 | tf_op jit(solution)/shard_map/ppermute | solution.py:385
  33.1 11.2 %collective-permute-start.20 = (bf16[32,2176]{1,0:T(8,128)(2,1)S(1)}, bf16[32,2176]{1,0:T(8,128)(2,1)S(1)}, u32[]{:S(2)}, u32[]{:S(2)}) collective-permute-start(bf16[32,2176]{1,0:T(8,128)(2,1)S(1)} %get-tuple-element.119), channel_id=1, source_target_pairs={{0,7},{1,6},{2,5},{3,4},{4,3},{5,2},{6,1},{7,0},{8,15},{9,14},{10,... | collective-permute-start | bytes 417800 | tf_op jit(solution)/shard_map/ppermute | solution.py:381
  34.9 16.3 %collective-permute-start.35 = (bf16[48,2048]{1,0:T(8,128)(2,1)S(1)}, bf16[48,2048]{1,0:T(8,128)(2,1)S(1)}, u32[]{:S(2)}, u32[]{:S(2)}) collective-permute-start(bf16[48,2048]{1,0:T(8,128)(2,1)S(1)} %get-tuple-element.140), channel_id=1, source_target_pairs={{0,8},{1,9},{2,10},{3,11},{4,12},{5,13},{6,14},{7,15},{8,16},{9,17... | collective-permute-start | bytes 589832 | tf_op jit(solution)/shard_map/ppermute | solution.py:385
  37.4 10.7 %collective-permute-start.21 = (bf16[32,2176]{1,0:T(8,128)(2,1)S(1)}, bf16[32,2176]{1,0:T(8,128)(2,1)S(1)}, u32[]{:S(2)}, u32[]{:S(2)}) collective-permute-start(bf16[32,2176]{1,0:T(8,128)(2,1)S(1)} %get-tuple-element.121), channel_id=1, source_target_pairs={{0,1},{1,0},{2,3},{3,2},{4,5},{5,4},{6,7},{7,6},{8,9},{9,8},{10,11... | collective-permute-start | bytes 417800 | tf_op jit(solution)/shard_map/ppermute | solution.py:381
  44.2 13.4 %collective-permute-start.36 = (bf16[48,2048]{1,0:T(8,128)(2,1)S(1)}, bf16[48,2048]{1,0:T(8,128)(2,1)S(1)}, u32[]{:S(2)}, u32[]{:S(2)}) collective-permute-start(bf16[48,2048]{1,0:T(8,128)(2,1)S(1)} %get-tuple-element.141), channel_id=1, source_target_pairs={{0,16},{1,17},{2,18},{3,19},{4,20},{5,21},{6,22},{7,23},{8,24},{9,... | collective-permute-start | bytes 589832 | tf_op jit(solution)/shard_map/ppermute | solution.py:385
  48.2 13.7 %collective-permute-start.3 = (bf16[48,2048]{1,0:T(8,128)(2,1)S(1)}, bf16[48,2048]{1,0:T(8,128)(2,1)S(1)}, u32[]{:S(2)}, u32[]{:S(2)}) collective-permute-start(bf16[48,2048]{1,0:T(8,128)(2,1)S(1)} %get-tuple-element.96), channel_id=1, source_target_pairs={{0,24},{1,25},{2,26},{3,27},{4,28},{5,29},{6,30},{7,31},{8,0},{9,1... | collective-permute-start | bytes 589832 | tf_op jit(solution)/shard_map/ppermute | solution.py:385
  64.4 11.8 %collective-permute-start.41 = (bf16[32,2048]{1,0:T(8,128)(2,1)S(1)}, bf16[32,2048]{1,0:T(8,128)(2,1)S(1)}, u32[]{:S(2)}, u32[]{:S(2)}) collective-permute-start(bf16[32,2048]{1,0:T(8,128)(2,1)S(1)} %get-tuple-element.149), channel_id=1, source_target_pairs={{0,5},{1,4},{2,7},{3,6},{4,1},{5,0},{6,3},{7,2},{8,13},{9,12},{10,... | collective-permute-start | bytes 393224 | tf_op jit(solution)/shard_map/ppermute | solution.py:381
  64.5 12.6 %collective-permute-start.42 = (bf16[32,2048]{1,0:T(8,128)(2,1)S(1)}, bf16[32,2048]{1,0:T(8,128)(2,1)S(1)}, u32[]{:S(2)}, u32[]{:S(2)}) collective-permute-start(bf16[32,2048]{1,0:T(8,128)(2,1)S(1)} %get-tuple-element.150), channel_id=1, source_target_pairs={{0,6},{1,7},{2,4},{3,5},{4,2},{5,3},{6,0},{7,1},{8,14},{9,15},{10,... | collective-permute-start | bytes 393224 | tf_op jit(solution)/shard_map/ppermute | solution.py:381
  84.6 11.7 %collective-permute-start.44 = (bf16[32,2176]{1,0:T(8,128)(2,1)S(1)}, bf16[32,2176]{1,0:T(8,128)(2,1)S(1)}, u32[]{:S(2)}, u32[]{:S(2)}) collective-permute-start(bf16[32,2176]{1,0:T(8,128)(2,1)S(1)} %get-tuple-element.153), channel_id=1, source_target_pairs={{0,1},{1,0},{2,3},{3,2},{4,5},{5,4},{6,7},{7,6},{8,9},{9,8},{10,11... | collective-permute-start | bytes 417800 | tf_op jit(solution)/shard_map/ppermute | solution.py:381
  85.2 12.6 %collective-permute-start.45 = (bf16[32,2176]{1,0:T(8,128)(2,1)S(1)}, bf16[32,2176]{1,0:T(8,128)(2,1)S(1)}, u32[]{:S(2)}, u32[]{:S(2)}) collective-permute-start(bf16[32,2176]{1,0:T(8,128)(2,1)S(1)} %get-tuple-element.154), channel_id=1, source_target_pairs={{0,2},{1,3},{2,0},{3,1},{4,6},{5,7},{6,4},{7,5},{8,10},{9,11},{10,... | collective-permute-start | bytes 417800 | tf_op jit(solution)/shard_map/ppermute | solution.py:381
  98.3 11.3 %collective-permute-start.33 = (bf16[32,2176]{1,0:T(8,128)(2,1)S(1)}, bf16[32,2176]{1,0:T(8,128)(2,1)S(1)}, u32[]{:S(2)}, u32[]{:S(2)}) collective-permute-start(bf16[32,2176]{1,0:T(8,128)(2,1)S(1)} %get-tuple-element.137), channel_id=1, source_target_pairs={{0,6},{1,7},{2,4},{3,5},{4,2},{5,3},{6,0},{7,1},{8,14},{9,15},{10,... | collective-permute-start | bytes 417800 | tf_op jit(solution)/shard_map/ppermute | solution.py:381
  102.8 11.5 %collective-permute-start.46 = (bf16[32,2176]{1,0:T(8,128)(2,1)S(1)}, bf16[32,2176]{1,0:T(8,128)(2,1)S(1)}, u32[]{:S(2)}, u32[]{:S(2)}) collective-permute-start(bf16[32,2176]{1,0:T(8,128)(2,1)S(1)} %get-tuple-element.155), channel_id=1, source_target_pairs={{0,3},{1,2},{2,1},{3,0},{4,7},{5,6},{6,5},{7,4},{8,11},{9,10},{10,... | collective-permute-start | bytes 417800 | tf_op jit(solution)/shard_map/ppermute | solution.py:381
  104.4 13.4 %collective-permute-start.47 = (bf16[32,2176]{1,0:T(8,128)(2,1)S(1)}, bf16[32,2176]{1,0:T(8,128)(2,1)S(1)}, u32[]{:S(2)}, u32[]{:S(2)}) collective-permute-start(bf16[32,2176]{1,0:T(8,128)(2,1)S(1)} %get-tuple-element.156), channel_id=1, source_target_pairs={{0,4},{1,5},{2,6},{3,7},{4,0},{5,1},{6,2},{7,3},{8,12},{9,13},{10,... | collective-permute-start | bytes 417800 | tf_op jit(solution)/shard_map/ppermute | solution.py:381
  105.1 12.8 %collective-permute-start.48 = (bf16[32,2176]{1,0:T(8,128)(2,1)S(1)}, bf16[32,2176]{1,0:T(8,128)(2,1)S(1)}, u32[]{:S(2)}, u32[]{:S(2)}) collective-permute-start(bf16[32,2176]{1,0:T(8,128)(2,1)S(1)} %get-tuple-element.157), channel_id=1, source_target_pairs={{0,5},{1,4},{2,7},{3,6},{4,1},{5,0},{6,3},{7,2},{8,13},{9,12},{10,... | collective-permute-start | bytes 417800 | tf_op jit(solution)/shard_map/ppermute | solution.py:381
  109.6 11.9 %collective-permute-start.49 = (bf16[32,2176]{1,0:T(8,128)(2,1)S(1)}, bf16[32,2176]{1,0:T(8,128)(2,1)S(1)}, u32[]{:S(2)}, u32[]{:S(2)}) collective-permute-start(bf16[32,2176]{1,0:T(8,128)(2,1)S(1)} %get-tuple-element.158), channel_id=1, source_target_pairs={{0,6},{1,7},{2,4},{3,5},{4,2},{5,3},{6,0},{7,1},{8,14},{9,15},{10,... | collective-permute-start | bytes 417800 | tf_op jit(solution)/shard_map/ppermute | solution.py:381
  111.8 11.9 %collective-permute-start.50 = (bf16[32,2176]{1,0:T(8,128)(2,1)S(1)}, bf16[32,2176]{1,0:T(8,128)(2,1)S(1)}, u32[]{:S(2)}, u32[]{:S(2)}) collective-permute-start(bf16[32,2176]{1,0:T(8,128)(2,1)S(1)} %get-tuple-element.159), channel_id=1, source_target_pairs={{0,7},{1,6},{2,5},{3,4},{4,3},{5,2},{6,1},{7,0},{8,15},{9,14},{10,... | collective-permute-start | bytes 417800 | tf_op jit(solution)/shard_map/ppermute | solution.py:381
  114.2 23.9 %collective-permute-start.53 = (bf16[48,2176]{1,0:T(8,128)(2,1)S(1)}, bf16[48,2176]{1,0:T(8,128)(2,1)S(1)}, u32[]{:S(2)}, u32[]{:S(2)}) collective-permute-start(bf16[48,2176]{1,0:T(8,128)(2,1)S(1)} %get-tuple-element.162), channel_id=1, source_target_pairs={{0,8},{1,9},{2,10},{3,11},{4,12},{5,13},{6,14},{7,15},{8,16},{9,17... | collective-permute-start | bytes 626696 | tf_op jit(solution)/shard_map/ppermute | solution.py:385
  124.1 14.0 %collective-permute-start.51 = (bf16[48,2176]{1,0:T(8,128)(2,1)S(1)}, bf16[48,2176]{1,0:T(8,128)(2,1)S(1)}, u32[]{:S(2)}, u32[]{:S(2)}) collective-permute-start(bf16[48,2176]{1,0:T(8,128)(2,1)S(1)} %get-tuple-element.160), channel_id=1, source_target_pairs={{0,24},{1,25},{2,26},{3,27},{4,28},{5,29},{6,30},{7,31},{8,0},{9,1... | collective-permute-start | bytes 626696 | tf_op jit(solution)/shard_map/ppermute | solution.py:385
  130.7 12.8 %collective-permute-start.52 = (bf16[48,2176]{1,0:T(8,128)(2,1)S(1)}, bf16[48,2176]{1,0:T(8,128)(2,1)S(1)}, u32[]{:S(2)}, u32[]{:S(2)}) collective-permute-start(bf16[48,2176]{1,0:T(8,128)(2,1)S(1)} %get-tuple-element.161), channel_id=1, source_target_pairs={{0,16},{1,17},{2,18},{3,19},{4,20},{5,21},{6,22},{7,23},{8,24},{9,... | collective-permute-start | bytes 626696 | tf_op jit(solution)/shard_map/ppermute | solution.py:385
  (40 other events, 345.9 us)
where the time goes:
time: 145 us
  starting transfers between devices  67.4 us (46%)
  waiting for transfers between devices  45.7 us (32%)
  Pallas kernels  23.5 us (16%)
  local copies, waits for them, and re-layouts  7.21 us (5%)
    ppermute x42, starting transfers between devices, over_plane(): return lax.ppermute(array, AXES, pairs)  41.1 us
    ppermute x42, waiting for transfers between devices, over_plane(): return lax.ppermute(array, AXES, pairs)  24.6 us
    ppermute x9, starting transfers between devices, over_z(): return lax.ppermute(array, AXES, pairs)  24.4 us
    ppermute x9, waiting for transfers between devices, over_z(): return lax.ppermute(array, AXES, pairs)  21 us
    pallas_call x13, Pallas kernels, call(): pl.pallas_call(kernel, out_shape=outs, in_specs=[pl.BlockSpec(memory_spac...  16.1 us
    pallas_call x1, Pallas kernels, weight_call(): pl.pallas_call(functools.partial(weight_kernel, len(kept)), grid=(FEATURE...  7.4 us
    unnamed x20, local copies, waits for them, and re-layouts  7.21 us
  transfers between devices with their start and end apart: 54, of which 20 were waited for; matrix products, arithmetic and copies ran while one was open for 0% of the time, Pallas kernels for 15%

commit v1 on v0

--- a/solution.py
+++ b/solution.py
@@ -16,6 +16,8 @@
 FEATURE_TILES = 4
 SMALL_VMEM = 16 * 2**20
 BIG_VMEM = 24 * 2**20
+HEAD_VMEM = 60 * 2**20
+TOKEN_SETS = ((3, 0), (1, 2))
 SETS = ((1, 2), (3, 0))
 TOKEN_SHIFTS = (3, 1, 2)
 COT_SHIFTS = (1, 2, 3)
@@ -53,36 +55,39 @@
     return lax.div(flat, group_size), lax.rem(flat, group_size)
 
 
-def split_kernel(pieces, moe_ref, gain_ref, grad_ref, *out_refs):
+def head_kernel(pieces, group_size, share, *refs):
+    tok_hbm, routes_hbm, gates_hbm, moe_hbm, gain_hbm, grad_hbm = refs[:6]
+    part_refs, refs = refs[6 : 6 + pieces], refs[6 + pieces :]
+    out_refs, hot_ref = refs[:GROUPS], refs[GROUPS]
+    tok_ref, routes_ref, gates_ref, gain_ref, lines_ref, sems = refs[GROUPS + 1 :]
+    rows, features = tok_ref.shape
+    width = moe_hbm.shape[1]
     me = lax.axis_index("tp")
-    width = moe_ref.shape[1]
-    rows = moe_ref.shape[0] // pieces
-    gain = gain_ref[...]
-    high = gain.astype(BF).astype(F32)
-    middle = (gain - high).astype(BF).astype(F32)
-    low = gain - high - middle
-    line = lax.broadcasted_iota(jnp.int32, (GAIN_ROWS, width), 0)
-    parts = jnp.where(line == 0, high, jnp.where(line == 1, middle, 0.0))
-    parts = jnp.where(line == 2, low, parts).astype(BF)
-    for index in range(pieces):
-        first = pl.multiple_of(jnp.bitwise_xor(me, index) * rows, rows)
-        out_refs[index][:rows, :width] = grad_ref[pl.ds(first, rows), :]
-        out_refs[index][:rows, width:] = moe_ref[pl.ds(first, rows), :]
-        out_refs[index][rows:, :width] = parts
-        out_refs[index][rows:, width:] = jnp.zeros((GAIN_ROWS, width), BF)
-
-
-def token_pack_kernel(group_size, share, tok_ref, routes_ref, gates_ref, *refs):
-    out_refs, hot_ref, rows_ref = refs[:-2], refs[-2], refs[-1]
-    rows, features = tok_ref.shape
     plane, _ = place(group_size)
-    rows_ref[...] = jnp.zeros_like(rows_ref)
-    rows_ref[0:2, :] = routes_ref[...].astype(F32)
-    rows_ref[2:4, :] = gates_ref[...]
+
+    sources = [
+        (routes_hbm, routes_ref),
+        (gates_hbm, gates_ref),
+        (tok_hbm, tok_ref),
+        (gain_hbm, gain_ref),
+    ]
+    for index, ref in enumerate(part_refs):
+        block = pl.ds(pl.multiple_of(jnp.bitwise_xor(me, index) * rows, rows), rows)
+        sources.append((grad_hbm.at[block, :], ref.at[pl.ds(0, rows), pl.ds(0, width)]))
+        sources.append((moe_hbm.at[block, :], ref.at[pl.ds(0, rows), pl.ds(width, width)]))
+    copies = [pltpu.make_async_copy(a, b, sems.at[i]) for i, (a, b) in enumerate(sources)]
+    for copy in copies:
+        copy.start()
+
+    lines_ref[...] = jnp.zeros_like(lines_ref)
+    copies[0].wait()
+    copies[1].wait()
+    lines_ref[0:2, :] = routes_ref[...].astype(F32)
+    lines_ref[2:4, :] = gates_ref[...]
     unit_row = lax.broadcasted_iota(jnp.int32, (rows, rows), 0)
     unit_col = lax.broadcasted_iota(jnp.int32, (rows, rows), 1)
     unit = jnp.where(unit_row == unit_col, 1.0, 0.0).astype(BF)
-    columns = contract(unit, rows_ref[...].astype(BF), 1, 1)
+    columns = contract(unit, lines_ref[...].astype(BF), 1, 1)
     first = columns[:, 0:1].astype(jnp.int32)
     second = columns[:, 1:2].astype(jnp.int32)
     group = lax.div(first, group_size)
@@ -102,11 +107,26 @@
         ),
         rows,
     ).astype(BF)
+    packed_meta = contract(hot, meta, 0, 0).astype(BF)
+    copies[2].wait()
     packed = contract(hot, tok_ref[...], 0, 0).astype(BF)
-    packed_meta = contract(hot, meta, 0, 0).astype(BF)
     for index in range(GROUPS):
         out_refs[index][:, :features] = packed[index * share : (index + 1) * share]
         out_refs[index][:, features:] = packed_meta[index * share : (index + 1) * share]
+
+    copies[3].wait()
+    gain = gain_ref[...]
+    high = gain.astype(BF).astype(F32)
+    middle = (gain - high).astype(BF).astype(F32)
+    low = gain - high - middle
+    line = lax.broadcasted_iota(jnp.int32, (GAIN_ROWS, width), 0)
+    parts = jnp.where(line == 0, high, jnp.where(line == 1, middle, 0.0))
+    parts = jnp.where(line == 2, low, parts).astype(BF)
+    for ref in part_refs:
+        ref[rows:, :width] = parts
+        ref[rows:, width:] = jnp.zeros((GAIN_ROWS, width), BF)
+    for copy in copies[4:]:
+        copy.wait()
 
 
 def cot_pack_kernel(pieces, share, *refs):
@@ -138,10 +158,24 @@
         out_refs[index][...] = packed[index * share : (index + 1) * share]
 
 
-def token_route_kernel(group_size, capacity, *refs):
-    shifts = len(refs) - group_size - 3
+def route_hots(part_refs, group_size, capacity):
+    slots = len(part_refs) * capacity
+    hots = []
+    for k in range(2):
+        blocks = []
+        for index, ref in enumerate(part_refs):
+            part = ref[...].astype(F32)
+            partner = part[:, 2 * k : 2 * k + 1]
+            slot = partner * slots + index * capacity + part[:, 2 * k + 1 : 2 * k + 2]
+            slot = jnp.where(partner < 0, -1.0, slot).astype(jnp.int32)
+            blocks.append(one_hot(slot, group_size * slots))
+        hots.append(jnp.concatenate(blocks, axis=0))
+    return hots
+
+
+def token_route_kernel(shifts, group_size, capacity, *refs):
     msg_refs, out_refs = refs[:shifts], refs[shifts : shifts + group_size]
-    hot0_ref, hot1_ref, full_ref = refs[-3:]
+    part_refs, full_ref = refs[shifts + group_size : -1], refs[-1]
     share, width = msg_refs[0].shape
     features = width - META
     slots = shifts * capacity
@@ -156,12 +190,13 @@
         experts = [meta[:, k : k + 1].astype(jnp.int32) - 1 for k in range(2)]
         members = [one_hot(e, META) for e in experts]
         before = contract(lower, members[0] + members[1], 1, 0)
-        for expert, member, hot_ref in zip(experts, members, (hot0_ref, hot1_ref)):
-            rank = jnp.sum(before * member.astype(F32), axis=1, keepdims=True)
-            slot = jnp.bitwise_xor(expert, mine) * slots + index * capacity
-            slot = jnp.where(expert < 0, -1, slot + rank.astype(jnp.int32))
-            hot_ref[row, :] = one_hot(slot, group_size * slots)
-    hot0, hot1 = hot0_ref[...], hot1_ref[...]
+        parts = []
+        for expert, member in zip(experts, members):
+            partner = jnp.where(expert < 0, -1, jnp.bitwise_xor(expert, mine))
+            parts.append(partner.astype(F32))
+            parts.append(jnp.sum(before * member.astype(F32), axis=1, keepdims=True))
+        part_refs[index][...] = lane_of(parts, share).astype(BF)
+    hot0, hot1 = route_hots(part_refs, group_size, capacity)
     total = shifts * share
     gate0 = lane_of((jnp.concatenate([g[0] for g in gates], axis=0),), total).astype(BF)
     gate1 = lane_of((jnp.concatenate([g[1] for g in gates], axis=0),), total).astype(BF)
@@ -173,26 +208,26 @@
         out_refs[index][:, features:] = packed_gate[row].astype(BF)
 
 
-def cot_route_kernel(group_size, *refs):
-    shifts = len(refs) - group_size - 3
-    msg_refs, hot0_ref, hot1_ref = refs[:shifts], refs[shifts], refs[shifts + 1]
-    out_refs, full_ref = refs[shifts + 2 : -1], refs[-1]
+def cot_route_kernel(shifts, group_size, capacity, *refs):
+    msg_refs, part_refs = refs[:shifts], refs[shifts : 2 * shifts]
+    out_refs, full_ref = refs[2 * shifts : -1], refs[-1]
     share = msg_refs[0].shape[0]
-    slots = hot0_ref.shape[1] // group_size
+    slots = shifts * capacity
     for index, ref in enumerate(msg_refs):
         full_ref[index * share : (index + 1) * share, :] = ref[...]
-    packed = contract(hot0_ref[...] + hot1_ref[...], full_ref[...], 0, 0)
+    hot0, hot1 = route_hots(part_refs, group_size, capacity)
+    packed = contract(hot0 + hot1, full_ref[...], 0, 0)
     for index in range(group_size):
         out_refs[index][...] = packed[index * slots : (index + 1) * slots].astype(BF)
 
 
-def combine_kernel(group_size, shifts, *refs):
-    piece_refs, hot0_ref, hot1_ref = refs[:group_size], refs[group_size], refs[group_size + 1]
-    out_refs = refs[group_size + 2 :]
-    features = piece_refs[0].shape[1] - META
-    share = hot0_ref.shape[0] // shifts
+def combine_kernel(shifts, group_size, capacity, *refs):
+    piece_refs, part_refs = refs[:group_size], refs[group_size : group_size + shifts]
+    out_refs = refs[group_size + shifts :]
+    share, width = out_refs[0].shape
+    features = width - META
     rows = jnp.concatenate([ref[...].astype(F32) for ref in piece_refs], axis=0).astype(BF)
-    hot0, hot1 = hot0_ref[...], hot1_ref[...]
+    hot0, hot1 = route_hots(part_refs, group_size, capacity)
     summed = contract(hot0 + hot1, rows[:, :features], 1, 0).astype(BF)
     grad0 = contract(hot0, rows[:, features:], 1, 0)[:, 0:1]
     grad1 = contract(hot1, rows[:, features:], 1, 0)[:, 0:1]
@@ -217,19 +252,16 @@
     count = len(refs) - 6
     piece_refs, (gate_ref, up_ref) = refs[:count], refs[count : count + 2]
     rows_ref, meta_ref, pre_gate_ref, pre_up_ref = refs[count + 2 :]
-    features = rows_ref.shape[1]
-    first = 0
-    for ref in piece_refs:
-        last = first + ref.shape[0]
-        rows_ref[first:last, :] = ref[:, :features]
-        meta_ref[first:last, :] = ref[:, features:]
-        first = last
+    slots, features = piece_refs[0].shape[0], rows_ref.shape[1]
+    for index, ref in enumerate(piece_refs):
+        rows_ref[index * slots : (index + 1) * slots, :] = ref[:, :features]
+        meta_ref[index * slots : (index + 1) * slots, :] = ref[:, features:]
     rows = rows_ref[...]
     pre_gate_ref[...] = contract(rows, gate_ref[0], 1, 0)
     pre_up_ref[...] = contract(rows, up_ref[0], 1, 0)
 
 
-def backward_kernel(group_size, first, *refs):
+def backward_kernel(group_size, *refs):
     piece_refs = refs[:group_size]
     meta_ref, pre_gate_ref, pre_up_ref, gate_ref, up_ref, down_ref = refs[
         group_size : group_size + 6
@@ -238,12 +270,11 @@
     d_gate_ref, d_up_ref, hidden_ref, scaled_ref, cot_ref = refs[2 * group_size + 6 :]
     slots, features = piece_refs[0].shape
     rows = cot_ref.shape[0]
-    held = slice(first, first + rows)
     for index, ref in enumerate(piece_refs):
         cot_ref[index * slots : (index + 1) * slots, :] = ref[...]
-    weight = meta_ref[held, 0:1].astype(F32)
+    weight = meta_ref[:, 0:1].astype(F32)
     hid_grad = contract(cot_ref[...], down_ref[0], 1, 1)
-    pre_gate, pre_up = pre_gate_ref[held, :], pre_up_ref[held, :]
+    pre_gate, pre_up = pre_gate_ref[...], pre_up_ref[...]
     sigmoid_gate = jax.nn.sigmoid(pre_gate)
     activated = pre_gate * sigmoid_gate
     hidden = activated * pre_up
@@ -266,9 +297,9 @@
     scaled_ref[...] = (weight * cot_ref[...].astype(F32)).astype(BF)
 
 
-def weight_kernel(sets, rows_ref, *refs):
-    d_gate, d_up, hidden, scaled = (refs[k * sets : (k + 1) * sets] for k in range(4))
-    grad_gate_ref, grad_up_ref, grad_down_ref, both_ref, turned_ref = refs[4 * sets :]
+def weight_kernel(sets, *refs):
+    rows, d_gate, d_up, hidden, scaled = (refs[k * sets : (k + 1) * sets] for k in range(5))
+    grad_gate_ref, grad_up_ref, grad_down_ref, both_ref, turned_ref = refs[5 * sets :]
     hidden_width = hidden[0].shape[1]
 
     @pl.when(pl.program_id(0) == 0)
@@ -281,7 +312,8 @@
             turned_ref[:, first:last] = hid[...].T
             first = last
 
-    both = contract(rows_ref[...], both_ref[...], 0, 0)
+    tokens = jnp.concatenate([ref[...] for ref in rows], axis=0)
+    both = contract(tokens, both_ref[...], 0, 0)
     grad_gate_ref[0] = both[:, :hidden_width].astype(BF)
     grad_up_ref[0] = both[:, hidden_width:].astype(BF)
     cots = jnp.concatenate([ref[...] for ref in scaled], axis=0)
@@ -300,12 +332,12 @@
     )
 
 
-def backward_call(first, pieces, *held):
+def backward_call(pieces, *held):
     features, hidden = held[3].shape[1:]
     slots = pieces[0].shape[0]
     rows = slots * len(pieces)
     result = call(
-        functools.partial(backward_kernel, len(pieces), first),
+        functools.partial(backward_kernel, len(pieces)),
         [(slots, features + META)] * len(pieces) + [(rows, hidden)] * 3 + [(rows, features)],
         [*pieces, *held],
         scratch=[((rows, features), BF)],
@@ -317,7 +349,7 @@
 
 def weight_call(rows, kept):
     d_gate, d_up, hidden, scaled = ([k[i] for k in kept] for i in range(4))
-    total, features = rows.shape
+    total, features = sum(r.shape[0] for r in rows), rows[0].shape[1]
     width = hidden[0].shape[1]
     tile = features // FEATURE_TILES
     whole = lambda a: pl.BlockSpec(a.shape, lambda d: (0, 0))
@@ -329,7 +361,7 @@
             jax.ShapeDtypeStruct((1, features, width), BF),
             jax.ShapeDtypeStruct((1, width, features), BF),
         ],
-        in_specs=[pl.BlockSpec((total, tile), lambda d: (0, d))]
+        in_specs=[pl.BlockSpec((a.shape[0], tile), lambda d: (0, d)) for a in rows]
         + [whole(a) for a in (*d_gate, *d_up, *hidden)]
         + [pl.BlockSpec((a.shape[0], tile), lambda d: (0, d)) for a in scaled],
         out_specs=[
@@ -344,18 +376,19 @@
             bytes_accessed=6 * features * width + 4 * total * features + 6 * total * width,
             transcendentals=0,
         ),
-    )(rows, *d_gate, *d_up, *hidden, *scaled)
-
-
-def call(kernel, outs, args, scratch=(), flops=0, limit=SMALL_VMEM):
+    )(*rows, *d_gate, *d_up, *hidden, *scaled)
+
+
+def call(kernel, outs, args, scratch=(), copies=0, flops=0, limit=SMALL_VMEM):
     outs = [jax.ShapeDtypeStruct(o[:2], o[2] if len(o) > 2 else BF) for o in outs]
     size = sum(a.size * a.dtype.itemsize for a in (*args, *outs))
     return pl.pallas_call(
         kernel,
         out_shape=outs,
-        in_specs=[pl.BlockSpec(memory_space=pltpu.VMEM)] * len(args),
+        in_specs=[pl.BlockSpec(memory_space=pltpu.HBM if copies else pltpu.VMEM)] * len(args),
         out_specs=[pl.BlockSpec(memory_space=pltpu.VMEM)] * len(outs),
-        scratch_shapes=[pltpu.VMEM(shape, dtype) for shape, dtype in scratch],
+        scratch_shapes=[pltpu.VMEM(shape, dtype) for shape, dtype in scratch]
+        + [pltpu.SemaphoreType.DMA((copies,))] * bool(copies),
         compiler_params=pltpu.CompilerParams(vmem_limit_bytes=limit),
         cost_estimate=pl.CostEstimate(flops=flops, bytes_accessed=size, transcendentals=0),
     )(*args)
@@ -385,20 +418,26 @@
         return lax.ppermute(array, AXES, pairs)
 
     part = [(tok_rows + GAIN_ROWS, 2 * moe_out.shape[1])] * pieces
-    *tok_msgs, hot = call(
-        functools.partial(token_pack_kernel, group_size, share),
-        [(share, wide)] * GROUPS + [(tok_rows, GROUPS * share)],
-        (tokens, routes.T, gates.T),
-        scratch=[((8, tok_rows), F32)],
+    *out, hot = call(
+        functools.partial(head_kernel, pieces, group_size, share),
+        part + [(share, wide)] * GROUPS + [(tok_rows, GROUPS * share)],
+        (tokens, routes.T, gates.T, moe_out, norm_gain[None, :], out_grad),
+        scratch=[
+            ((tok_rows, features), BF),
+            (routes.shape[::-1], jnp.int32),
+            (gates.shape[::-1], F32),
+            ((1, norm_gain.shape[0]), F32),
+            ((8, tok_rows), F32),
+        ],
+        copies=4 + 2 * pieces,
+        limit=HEAD_VMEM,
         flops=2 * tok_rows * GROUPS * share * wide,
     )
+    split, tok_msgs = out[:pieces], out[pieces:]
+    split = [split[0]] + [over_tp(split[m], m) for m in range(1, pieces)]
     tok_at = {0: tok_msgs[0]}
     for s in TOKEN_SHIFTS:
         tok_at[s] = over_z(tok_msgs[s], s)
-    split = call(
-        functools.partial(split_kernel, pieces), part, (moe_out, norm_gain[None, :], out_grad)
-    )
-    split = [split[0]] + [over_tp(split[m], m) for m in range(1, pieces)]
     cot_msgs = call(
         functools.partial(cot_pack_kernel, pieces, share),
         [(share, features)] * GROUPS,
@@ -410,48 +449,48 @@
     for s in COT_SHIFTS:
         cot_at[s] = over_z(cot_msgs[s], s)
 
-    hots, tok_in, cot_in = [], [], []
-    for group in SETS:
+    parts, tok_in, cot_in = {}, [], []
+    for group in TOKEN_SETS:
         count = len(group)
         slots = count * capacity
-        *out, hot0, hot1 = call(
-            functools.partial(token_route_kernel, group_size, capacity),
-            [(slots, wide)] * group_size + [(count * share, group_size * slots)] * 2,
+        out = call(
+            functools.partial(token_route_kernel, count, group_size, capacity),
+            [(slots, wide)] * group_size + [(share, META)] * count,
             [tok_at[s] for s in group],
             scratch=[((count * share, features), BF)],
             flops=2 * count * share * group_size * slots * wide,
         )
-        hots.append((hot0, hot1))
+        parts.update(zip(group, out[group_size:]))
         tok_in.append([out[0]] + [over_plane(out[m], m) for m in range(1, group_size)])
-    for group, (hot0, hot1) in zip(SETS, hots):
+    for group in SETS:
         count = len(group)
         slots = count * capacity
         out = call(
-            functools.partial(cot_route_kernel, group_size),
+            functools.partial(cot_route_kernel, count, group_size, capacity),
             [(slots, features)] * group_size,
-            [cot_at[s] for s in group] + [hot0, hot1],
+            [cot_at[s] for s in group] + [parts[s] for s in group],
             scratch=[((count * share, features), BF)],
             flops=2 * count * share * group_size * slots * features,
         )
         cot_in.append([out[0]] + [over_plane(out[m], m) for m in range(1, group_size)])
 
-    row_block, meta, pre_gate, pre_up = forward_call([p for t in tok_in for p in t], w_gate, w_up)
-    backs, kept, first = [], [], 0
-    for cots in cot_in:
-        back, keep = backward_call(first, cots, meta, pre_gate, pre_up, w_gate, w_up, w_down)
-        first += cots[0].shape[0] * group_size
+    backs, kept, row_blocks = [], [], []
+    for group, cots in zip(SETS, cot_in):
+        rows, *held = forward_call(tok_in[TOKEN_SETS.index(group)], w_gate, w_up)
+        back, keep = backward_call(cots, *held, w_gate, w_up, w_down)
         backs.append([back[0]] + [over_plane(back[m], m) for m in range(1, group_size)])
         kept.append(keep)
-    grad_gate, grad_up, grad_down = weight_call(row_block, kept)
+        row_blocks.append(rows)
+    grad_gate, grad_up, grad_down = weight_call(row_blocks, kept)
 
     home = {}
-    for group, back, (hot0, hot1) in zip(SETS, backs, hots):
+    for group, back in zip(SETS, backs):
         count = len(group)
         out = call(
-            functools.partial(combine_kernel, group_size, count),
+            functools.partial(combine_kernel, count, group_size, capacity),
             [(share, wide)] * count,
-            [*back, hot0, hot1],
-            flops=2 * hot0.size * wide,
+            [*back] + [parts[s] for s in group],
+            flops=2 * count * share * group_size * count * capacity * wide,
         )
         for s, array in zip(group, out):
             home[s] = over_z(array, -s) if s else array

time: 145 us -> 142 us (0.979)
  starting transfers between devices: 67.4 us -> 62.4 us
  Pallas kernels: 23.5 us -> 26.7 us
  local copies, waits for them, and re-layouts: 7.21 us -> 4.63 us
    ppermute x9, starting transfers between devices: 24.4 us -> 18.5 us  [over_z(): return lax.ppermute(array, AXES, pairs)]
    ppermute x9, waiting for transfers between devices: 21 us -> 24.3 us  [over_z(): return lax.ppermute(array, AXES, pairs)]
    pallas_call x13, Pallas kernels: 16.1 us -> 19.3 us  [call(): pl.pallas_call(kernel, out_shape=outs, in_specs=[pl.BlockSpec(memory_spac...]
    unnamed x20 -> x14, local copies, waits for them, and re-layouts: 7.21 us -> 4.63 us
    ppermute x42, waiting for transfers between devices: 24.6 us -> 22.7 us  [over_plane(): return lax.ppermute(array, AXES, pairs)]
  transfers between devices with their start and end apart: 54 -> 54, of which waited for: 20 -> 17; matrix products, arithmetic and copies ran while one was open for 0% -> 0% of each run, Pallas kernels for 15% -> 16%
where the time goes in v1:
time: 142 us
  starting transfers between devices  62.4 us (44%)
  waiting for transfers between devices  47 us (33%)
  Pallas kernels  26.7 us (19%)
  local copies, waits for them, and re-layouts  4.63 us (3%)
    ppermute x42, starting transfers between devices, over_plane(): return lax.ppermute(array, AXES, pairs)  42 us
    ppermute x9, waiting for transfers between devices, over_z(): return lax.ppermute(array, AXES, pairs)  24.3 us
    ppermute x42, waiting for transfers between devices, over_plane(): return lax.ppermute(array, AXES, pairs)  22.7 us
    pallas_call x13, Pallas kernels, call(): pl.pallas_call(kernel, out_shape=outs, in_specs=[pl.BlockSpec(memory_spac...  19.3 us
    ppermute x9, starting transfers between devices, over_z(): return lax.ppermute(array, AXES, pairs)  18.5 us
    pallas_call x1, Pallas kernels, weight_call(): pl.pallas_call(functools.partial(weight_kernel, len(kept)), grid=(FEATURE...  7.42 us
    unnamed x14, local copies, waits for them, and re-layouts  4.63 us
  transfers between devices with their start and end apart: 54, of which 17 were waited for; matrix products, arithmetic and copies ran while one was open for 0% of the time, Pallas kernels for 16%

profile of v1, /device:TPU:0, one launch (start us, length us, event | category | flops | bytes accessed | tf_op | source)
XLA Modules:
  0.0 141.6 jit_solution(10826432428838813063)
XLA Ops:
  0.6 3.3 %shard_map.128 = (bf16[144,1024]{1,0:T(8,128)(2,1)}, bf16[144,1024]{1,0:T(8,128)(2,1)}, bf16[144,1024]{1,0:T(8,128)(2,1)}, bf16[144,1024]{1,0:T(8,128)(2,1)}, bf...) custom-call(bf16[128,2048]{1,0:T(8,128)(2,1)} %refs_0_.1, ...), custom_call_target="tpu_custom_call" | custom-call | flops 106954752 | bytes 3641344 | tf_op jit(solution)/shard_map/pallas_call | solution.py:385
  4.0 3.1 %collective-permute-start.28 = (bf16[48,2176]{1,0:T(8,128)(2,1)}, bf16[48,2176]{1,0:T(8,128)(2,1)S(1)}, u32[]{:S(2)}, u32[]{:S(2)}) collective-permute-start(bf16[48,2176]{1,0:T(8,128)(2,1)} %get-tuple-element.136), channel_id=1, source_target_pairs={{0,8},{1,9},{2,10},{3,11},{4,12},{5,13},{6,14},{7,15},{8,16},{9,17... | collective-permute-start | bytes 626696 | tf_op jit(solution)/shard_map/ppermute | solution.py:418
  7.1 2.6 %collective-permute-start.29 = (bf16[48,2176]{1,0:T(8,128)(2,1)}, bf16[48,2176]{1,0:T(8,128)(2,1)S(1)}, u32[]{:S(2)}, u32[]{:S(2)}) collective-permute-start(bf16[48,2176]{1,0:T(8,128)(2,1)} %get-tuple-element.137), channel_id=1, source_target_pairs={{0,16},{1,17},{2,18},{3,19},{4,20},{5,21},{6,22},{7,23},{8,24},{9,... | collective-permute-start | bytes 626696 | tf_op jit(solution)/shard_map/ppermute | solution.py:418
  11.6 3.9 %collective-permute-done.28.refs_0_ = bf16[48,2176]{1,0:T(8,128)(2,1)S(1)} collective-permute-done((bf16[48,2176]{1,0:T(8,128)(2,1)}, bf16[48,2176]{1,0:T(8,128)(2,1)S(1)}, u32[]{:S(2)}, u32[]{:S(2)}) %collective-permute-start.28) | collective-permute-done | bytes 208928 | tf_op jit(solution)/shard_map/ppermute | solution.py:418
  16.6 6.9 %collective-permute-done.29.refs_1_ = bf16[48,2176]{1,0:T(8,128)(2,1)S(1)} collective-permute-done((bf16[48,2176]{1,0:T(8,128)(2,1)}, bf16[48,2176]{1,0:T(8,128)(2,1)S(1)}, u32[]{:S(2)}, u32[]{:S(2)}) %collective-permute-start.29) | collective-permute-done | bytes 208928 | tf_op jit(solution)/shard_map/ppermute | solution.py:418
  24.6 2.9 %collective-permute-done.4.refs_0_ = bf16[48,2176]{1,0:T(8,128)(2,1)S(1)} collective-permute-done((bf16[48,2176]{1,0:T(8,128)(2,1)}, bf16[48,2176]{1,0:T(8,128)(2,1)S(1)}, u32[]{:S(2)}, u32[]{:S(2)}) %collective-permute-start.4) | collective-permute-done | bytes 208928 | tf_op jit(solution)/shard_map/ppermute | solution.py:418
  31.0 2.4 %collective-permute-start.42 = (bf16[32,2176]{1,0:T(8,128)(2,1)S(1)}, bf16[32,2176]{1,0:T(8,128)(2,1)S(1)}, u32[]{:S(2)}, u32[]{:S(2)}) collective-permute-start(bf16[32,2176]{1,0:T(8,128)(2,1)S(1)} %get-tuple-element.154), channel_id=1, source_target_pairs={{0,6},{1,7},{2,4},{3,5},{4,2},{5,3},{6,0},{7,1},{8,14},{9,15},{10,... | collective-permute-start | bytes 417800 | tf_op jit(solution)/shard_map/ppermute | solution.py:414
  36.1 3.3 %collective-permute-start.3 = (bf16[48,2048]{1,0:T(8,128)(2,1)S(1)}, bf16[48,2048]{1,0:T(8,128)(2,1)S(1)}, u32[]{:S(2)}, u32[]{:S(2)}) collective-permute-start(bf16[48,2048]{1,0:T(8,128)(2,1)S(1)} %get-tuple-element.100), channel_id=1, source_target_pairs={{0,24},{1,25},{2,26},{3,27},{4,28},{5,29},{6,30},{7,31},{8,0},{9,1... | collective-permute-start | bytes 589832 | tf_op jit(solution)/shard_map/ppermute | solution.py:418
  39.4 2.6 %collective-permute-start.27 = (bf16[48,2048]{1,0:T(8,128)(2,1)S(1)}, bf16[48,2048]{1,0:T(8,128)(2,1)S(1)}, u32[]{:S(2)}, u32[]{:S(2)}) collective-permute-start(bf16[48,2048]{1,0:T(8,128)(2,1)S(1)} %get-tuple-element.135), channel_id=1, source_target_pairs={{0,16},{1,17},{2,18},{3,19},{4,20},{5,21},{6,22},{7,23},{8,24},{9,... | collective-permute-start | bytes 589832 | tf_op jit(solution)/shard_map/ppermute | solution.py:418
  45.9 4.8 %collective-permute-done.13.refs_2_ = bf16[32,2176]{1,0:T(8,128)(2,1)S(1)} collective-permute-done((bf16[32,2176]{1,0:T(8,128)(2,1)S(1)}, bf16[32,2176]{1,0:T(8,128)(2,1)S(1)}, u32[]{:S(2)}, u32[]{:S(2)}) %collective-permute-start.13) | collective-permute-done | bytes 139296 | tf_op jit(solution)/shard_map/ppermute | solution.py:414
  52.7 3.9 %collective-permute-done.27.refs_1_ = bf16[48,2048]{1,0:T(8,128)(2,1)S(1)} collective-permute-done((bf16[48,2048]{1,0:T(8,128)(2,1)S(1)}, bf16[48,2048]{1,0:T(8,128)(2,1)S(1)}, u32[]{:S(2)}, u32[]{:S(2)}) %collective-permute-start.27) | collective-permute-done | bytes 196640 | tf_op jit(solution)/shard_map/ppermute | solution.py:418
  58.4 2.2 %collective-permute-start.43 = (bf16[32,2176]{1,0:T(8,128)(2,1)S(1)}, bf16[32,2176]{1,0:T(8,128)(2,1)S(1)}, u32[]{:S(2)}, u32[]{:S(2)}) collective-permute-start(bf16[32,2176]{1,0:T(8,128)(2,1)S(1)} %get-tuple-element.155), channel_id=1, source_target_pairs={{0,7},{1,6},{2,5},{3,4},{4,3},{5,2},{6,1},{7,0},{8,15},{9,14},{10,... | collective-permute-start | bytes 417800 | tf_op jit(solution)/shard_map/ppermute | solution.py:414
  68.7 2.2 %collective-permute-start.7 = (bf16[32,2048]{1,0:T(8,128)(2,1)S(1)}, bf16[32,2048]{1,0:T(8,128)(2,1)S(1)}, u32[]{:S(2)}, u32[]{:S(2)}) collective-permute-start(bf16[32,2048]{1,0:T(8,128)(2,1)S(1)} %get-tuple-element.109), channel_id=1, source_target_pairs={{0,3},{1,2},{2,1},{3,0},{4,7},{5,6},{6,5},{7,4},{8,11},{9,10},{10,... | collective-permute-start | bytes 393224 | tf_op jit(solution)/shard_map/ppermute | solution.py:414
  80.2 3.7 %collective-permute-done.10.refs_6_ = bf16[32,2048]{1,0:T(8,128)(2,1)S(1)} collective-permute-done((bf16[32,2048]{1,0:T(8,128)(2,1)S(1)}, bf16[32,2048]{1,0:T(8,128)(2,1)S(1)}, u32[]{:S(2)}, u32[]{:S(2)}) %collective-permute-start.10) | collective-permute-done | bytes 131104 | tf_op jit(solution)/shard_map/ppermute | solution.py:414
  83.9 2.1 %collective-permute-start.36 = (bf16[32,2048]{1,0:T(8,128)(2,1)S(1)}, bf16[32,2048]{1,0:T(8,128)(2,1)S(1)}, u32[]{:S(2)}, u32[]{:S(2)}) collective-permute-start(bf16[32,2048]{1,0:T(8,128)(2,1)S(1)} %get-tuple-element.147), channel_id=1, source_target_pairs={{0,7},{1,6},{2,5},{3,4},{4,3},{5,2},{6,1},{7,0},{8,15},{9,14},{10,... | collective-permute-start | bytes 393224 | tf_op jit(solution)/shard_map/ppermute | solution.py:414
  86.1 3.1 %shard_map.133 = (bf16[32,2176]{1,0:T(8,128)(2,1)S(1)}, bf16[32,2176]{1,0:T(8,128)(2,1)S(1)}, bf16[32,2176]{1,0:T(8,128)(2,1)S(1)}, bf16[32,2176]{1,0:T(8,128)(2...) custom-call(bf16[32,2048]{1,0:T(8,128)(2,1)S(1)} %get-tuple-element., ...), custom_call_target="tpu_custom_call" | custom-call | flops 2415919104 | bytes 15466496 | tf_op jit(solution)/shard_map/pallas_call | solution.py:385
  96.3 3.0 %shard_map.138 = (bf16[32,2176]{1,0:T(8,128)(2,1)S(1)}, bf16[32,2176]{1,0:T(8,128)(2,1)S(1)}, bf16[32,2176]{1,0:T(8,128)(2,1)S(1)}, bf16[32,2176]{1,0:T(8,128)(2...) custom-call(bf16[32,2048]{1,0:T(8,128)(2,1)S(1)} %get-tuple-element., ...), custom_call_target="tpu_custom_call" | custom-call | flops 2415919104 | bytes 15466496 | tf_op jit(solution)/shard_map/pallas_call | solution.py:385
  99.4 3.1 %collective-permute-start.24 = (bf16[32,2176]{1,0:T(8,128)(2,1)S(1)}, bf16[32,2176]{1,0:T(8,128)(2,1)S(1)}, u32[]{:S(2)}, u32[]{:S(2)}) collective-permute-start(bf16[32,2176]{1,0:T(8,128)(2,1)S(1)} %get-tuple-element.131), channel_id=1, source_target_pairs={{0,6},{1,7},{2,4},{3,5},{4,2},{5,3},{6,0},{7,1},{8,14},{9,15},{10,... | collective-permute-start | bytes 417800 | tf_op jit(solution)/shard_map/ppermute | solution.py:414
  104.5 2.2 %collective-permute-done.24.refs_6_ = bf16[32,2176]{1,0:T(8,128)(2,1)S(1)} collective-permute-done((bf16[32,2176]{1,0:T(8,128)(2,1)S(1)}, bf16[32,2176]{1,0:T(8,128)(2,1)S(1)}, u32[]{:S(2)}, u32[]{:S(2)}) %collective-permute-start.24) | collective-permute-done | bytes 139296 | tf_op jit(solution)/shard_map/ppermute | solution.py:414
  109.5 2.5 %collective-permute-start.49 = (bf16[32,2176]{1,0:T(8,128)(2,1)S(1)}, bf16[32,2176]{1,0:T(8,128)(2,1)S(1)}, u32[]{:S(2)}, u32[]{:S(2)}) collective-permute-start(bf16[32,2176]{1,0:T(8,128)(2,1)S(1)} %get-tuple-element.165), channel_id=1, source_target_pairs={{0,6},{1,7},{2,4},{3,5},{4,2},{5,3},{6,0},{7,1},{8,14},{9,15},{10,... | collective-permute-start | bytes 417800 | tf_op jit(solution)/shard_map/ppermute | solution.py:414
  119.5 2.6 %collective-permute-done.50.refs_7_ = bf16[32,2176]{1,0:T(8,128)(2,1)S(1)} collective-permute-done((bf16[32,2176]{1,0:T(8,128)(2,1)S(1)}, bf16[32,2176]{1,0:T(8,128)(2,1)S(1)}, u32[]{:S(2)}, u32[]{:S(2)}) %collective-permute-start.50) | collective-permute-done | bytes 139296 | tf_op jit(solution)/shard_map/ppermute | solution.py:414
  123.4 3.0 %collective-permute-start.52 = (bf16[48,2176]{1,0:T(8,128)(2,1)S(1)}, bf16[48,2176]{1,0:T(8,128)(2,1)S(1)}, u32[]{:S(2)}, u32[]{:S(2)}) collective-permute-start(bf16[48,2176]{1,0:T(8,128)(2,1)S(1)} %get-tuple-element.168), channel_id=1, source_target_pairs={{0,16},{1,17},{2,18},{3,19},{4,20},{5,21},{6,22},{7,23},{8,24},{9,... | collective-permute-start | bytes 626696 | tf_op jit(solution)/shard_map/ppermute | solution.py:418
  126.4 7.4 %shard_map.141 = (bf16[1,2048,768]{2,1,0:T(8,128)(2,1)}, bf16[1,2048,768]{2,1,0:T(8,128)(2,1)}, bf16[1,768,2048]{2,1,0:T(8,128)(2,1)}) custom-call(bf16[256,2048]{1,0:T(8,128)(2,1)S(1)} %get-tuple-element.172.refs_0_, bf16[256,2048]{1,0:T(8,128)(2,1)S(1)} %get-tuple-element.173.refs_1_, bf16[256,768]{1,0:T(8,128)(2,1)S(1)} %get-tuple-element.174.refs_2_, ...), custom_call_target="tpu_custom_call" | custom-call | flops 4831838208 | bytes 15990784 | tf_op jit(solution)/shard_map/pallas_call | solution.py:356
  133.8 6.7 %collective-permute-done.52.refs_2_ = bf16[48,2176]{1,0:T(8,128)(2,1)S(1)} collective-permute-done((bf16[48,2176]{1,0:T(8,128)(2,1)S(1)}, bf16[48,2176]{1,0:T(8,128)(2,1)S(1)}, u32[]{:S(2)}, u32[]{:S(2)}) %collective-permute-start.52) | collective-permute-done | bytes 208928 | tf_op jit(solution)/shard_map/ppermute | solution.py:418
  (112 shorter events, 57.0 us)
Async XLA Ops:
  4.0 11.5 %collective-permute-start.28 = (bf16[48,2176]{1,0:T(8,128)(2,1)}, bf16[48,2176]{1,0:T(8,128)(2,1)S(1)}, u32[]{:S(2)}, u32[]{:S(2)}) collective-permute-start(bf16[48,2176]{1,0:T(8,128)(2,1)} %get-tuple-element.136), channel_id=1, source_target_pairs={{0,8},{1,9},{2,10},{3,11},{4,12},{5,13},{6,14},{7,15},{8,16},{9,17... | collective-permute-start | bytes 626696 | tf_op jit(solution)/shard_map/ppermute | solution.py:418
  7.1 16.4 %collective-permute-start.29 = (bf16[48,2176]{1,0:T(8,128)(2,1)}, bf16[48,2176]{1,0:T(8,128)(2,1)S(1)}, u32[]{:S(2)}, u32[]{:S(2)}) collective-permute-start(bf16[48,2176]{1,0:T(8,128)(2,1)} %get-tuple-element.137), channel_id=1, source_target_pairs={{0,16},{1,17},{2,18},{3,19},{4,20},{5,21},{6,22},{7,23},{8,24},{9,... | collective-permute-start | bytes 626696 | tf_op jit(solution)/shard_map/ppermute | solution.py:418
  9.7 19.3 %collective-permute-start = (bf16[144,1024]{1,0:T(8,128)(2,1)}, bf16[144,1024]{1,0:T(8,128)(2,1)S(1)}, u32[]{:S(2)}, u32[]{:S(2)}) collective-permute-start(bf16[144,1024]{1,0:T(8,128)(2,1)} %get-tuple-element.97), channel_id=1, source_target_pairs={{0,1},{1,0},{2,3},{3,2},{4,5},{5,4},{6,7},{7,6},{8,9},{9,8},{10,11... | collective-permute-start | bytes 884744 | tf_op jit(solution)/shard_map/ppermute | solution.py:408
  9.7 19.3 %collective-permute-start.1 = (bf16[144,1024]{1,0:T(8,128)(2,1)}, bf16[144,1024]{1,0:T(8,128)(2,1)S(1)}, u32[]{:S(2)}, u32[]{:S(2)}) collective-permute-start(bf16[144,1024]{1,0:T(8,128)(2,1)} %get-tuple-element.98), channel_id=1, source_target_pairs={{0,2},{1,3},{2,0},{3,1},{4,6},{5,7},{6,4},{7,5},{8,10},{9,11},{10,... | collective-permute-start | bytes 884744 | tf_op jit(solution)/shard_map/ppermute | solution.py:408
  11.2 19.4 %collective-permute-start.2 = (bf16[144,1024]{1,0:T(8,128)(2,1)}, bf16[144,1024]{1,0:T(8,128)(2,1)S(1)}, u32[]{:S(2)}, u32[]{:S(2)}) collective-permute-start(bf16[144,1024]{1,0:T(8,128)(2,1)} %get-tuple-element.99), channel_id=1, source_target_pairs={{0,3},{1,2},{2,1},{3,0},{4,7},{5,6},{6,5},{7,4},{8,11},{9,10},{10,... | collective-permute-start | bytes 884744 | tf_op jit(solution)/shard_map/ppermute | solution.py:408
  15.5 12.0 %collective-permute-start.4 = (bf16[48,2176]{1,0:T(8,128)(2,1)}, bf16[48,2176]{1,0:T(8,128)(2,1)S(1)}, u32[]{:S(2)}, u32[]{:S(2)}) collective-permute-start(bf16[48,2176]{1,0:T(8,128)(2,1)} %get-tuple-element.102), channel_id=1, source_target_pairs={{0,24},{1,25},{2,26},{3,27},{4,28},{5,29},{6,30},{7,31},{8,0},{9,1... | collective-permute-start | bytes 626696 | tf_op jit(solution)/shard_map/ppermute | solution.py:418
  30.6 13.4 %collective-permute-start.41 = (bf16[32,2176]{1,0:T(8,128)(2,1)S(1)}, bf16[32,2176]{1,0:T(8,128)(2,1)S(1)}, u32[]{:S(2)}, u32[]{:S(2)}) collective-permute-start(bf16[32,2176]{1,0:T(8,128)(2,1)S(1)} %get-tuple-element.153), channel_id=1, source_target_pairs={{0,5},{1,4},{2,7},{3,6},{4,1},{5,0},{6,3},{7,2},{8,13},{9,12},{10,... | collective-permute-start | bytes 417800 | tf_op jit(solution)/shard_map/ppermute | solution.py:414
  31.0 13.1 %collective-permute-start.42 = (bf16[32,2176]{1,0:T(8,128)(2,1)S(1)}, bf16[32,2176]{1,0:T(8,128)(2,1)S(1)}, u32[]{:S(2)}, u32[]{:S(2)}) collective-permute-start(bf16[32,2176]{1,0:T(8,128)(2,1)S(1)} %get-tuple-element.154), channel_id=1, source_target_pairs={{0,6},{1,7},{2,4},{3,5},{4,2},{5,3},{6,0},{7,1},{8,14},{9,15},{10,... | collective-permute-start | bytes 417800 | tf_op jit(solution)/shard_map/ppermute | solution.py:414
  36.1 15.1 %collective-permute-start.3 = (bf16[48,2048]{1,0:T(8,128)(2,1)S(1)}, bf16[48,2048]{1,0:T(8,128)(2,1)S(1)}, u32[]{:S(2)}, u32[]{:S(2)}) collective-permute-start(bf16[48,2048]{1,0:T(8,128)(2,1)S(1)} %get-tuple-element.100), channel_id=1, source_target_pairs={{0,24},{1,25},{2,26},{3,27},{4,28},{5,29},{6,30},{7,31},{8,0},{9,1... | collective-permute-start | bytes 589832 | tf_op jit(solution)/shard_map/ppermute | solution.py:418
  39.4 11.8 %collective-permute-start.26 = (bf16[48,2048]{1,0:T(8,128)(2,1)S(1)}, bf16[48,2048]{1,0:T(8,128)(2,1)S(1)}, u32[]{:S(2)}, u32[]{:S(2)}) collective-permute-start(bf16[48,2048]{1,0:T(8,128)(2,1)S(1)} %get-tuple-element.134), channel_id=1, source_target_pairs={{0,8},{1,9},{2,10},{3,11},{4,12},{5,13},{6,14},{7,15},{8,16},{9,17... | collective-permute-start | bytes 589832 | tf_op jit(solution)/shard_map/ppermute | solution.py:418
  39.4 17.3 %collective-permute-start.27 = (bf16[48,2048]{1,0:T(8,128)(2,1)S(1)}, bf16[48,2048]{1,0:T(8,128)(2,1)S(1)}, u32[]{:S(2)}, u32[]{:S(2)}) collective-permute-start(bf16[48,2048]{1,0:T(8,128)(2,1)S(1)} %get-tuple-element.135), channel_id=1, source_target_pairs={{0,16},{1,17},{2,18},{3,19},{4,20},{5,21},{6,22},{7,23},{8,24},{9,... | collective-permute-start | bytes 589832 | tf_op jit(solution)/shard_map/ppermute | solution.py:418
  45.4 13.0 %collective-permute-start.14 = (bf16[32,2176]{1,0:T(8,128)(2,1)S(1)}, bf16[32,2176]{1,0:T(8,128)(2,1)S(1)}, u32[]{:S(2)}, u32[]{:S(2)}) collective-permute-start(bf16[32,2176]{1,0:T(8,128)(2,1)S(1)} %get-tuple-element.117), channel_id=1, source_target_pairs={{0,3},{1,2},{2,1},{3,0},{4,7},{5,6},{6,5},{7,4},{8,11},{9,10},{10,... | collective-permute-start | bytes 417800 | tf_op jit(solution)/shard_map/ppermute | solution.py:414
  51.2 11.5 %collective-permute-start.17 = (bf16[32,2176]{1,0:T(8,128)(2,1)S(1)}, bf16[32,2176]{1,0:T(8,128)(2,1)S(1)}, u32[]{:S(2)}, u32[]{:S(2)}) collective-permute-start(bf16[32,2176]{1,0:T(8,128)(2,1)S(1)} %get-tuple-element.120), channel_id=1, source_target_pairs={{0,6},{1,7},{2,4},{3,5},{4,2},{5,3},{6,0},{7,1},{8,14},{9,15},{10,... | collective-permute-start | bytes 417800 | tf_op jit(solution)/shard_map/ppermute | solution.py:414
  72.3 11.7 %collective-permute-start.10 = (bf16[32,2048]{1,0:T(8,128)(2,1)S(1)}, bf16[32,2048]{1,0:T(8,128)(2,1)S(1)}, u32[]{:S(2)}, u32[]{:S(2)}) collective-permute-start(bf16[32,2048]{1,0:T(8,128)(2,1)S(1)} %get-tuple-element.112), channel_id=1, source_target_pairs={{0,6},{1,7},{2,4},{3,5},{4,2},{5,3},{6,0},{7,1},{8,14},{9,15},{10,... | collective-permute-start | bytes 393224 | tf_op jit(solution)/shard_map/ppermute | solution.py:414
  77.2 12.0 %collective-permute-start.32 = (bf16[32,2048]{1,0:T(8,128)(2,1)S(1)}, bf16[32,2048]{1,0:T(8,128)(2,1)S(1)}, u32[]{:S(2)}, u32[]{:S(2)}) collective-permute-start(bf16[32,2048]{1,0:T(8,128)(2,1)S(1)} %get-tuple-element.143), channel_id=1, source_target_pairs={{0,3},{1,2},{2,1},{3,0},{4,7},{5,6},{6,5},{7,4},{8,11},{9,10},{10,... | collective-permute-start | bytes 393224 | tf_op jit(solution)/shard_map/ppermute | solution.py:414
  77.3 12.8 %collective-permute-start.33 = (bf16[32,2048]{1,0:T(8,128)(2,1)S(1)}, bf16[32,2048]{1,0:T(8,128)(2,1)S(1)}, u32[]{:S(2)}, u32[]{:S(2)}) collective-permute-start(bf16[32,2048]{1,0:T(8,128)(2,1)S(1)} %get-tuple-element.144), channel_id=1, source_target_pairs={{0,4},{1,5},{2,6},{3,7},{4,0},{5,1},{6,2},{7,3},{8,12},{9,13},{10,... | collective-permute-start | bytes 393224 | tf_op jit(solution)/shard_map/ppermute | solution.py:414
  79.1 11.6 %collective-permute-start.34 = (bf16[32,2048]{1,0:T(8,128)(2,1)S(1)}, bf16[32,2048]{1,0:T(8,128)(2,1)S(1)}, u32[]{:S(2)}, u32[]{:S(2)}) collective-permute-start(bf16[32,2048]{1,0:T(8,128)(2,1)S(1)} %get-tuple-element.145), channel_id=1, source_target_pairs={{0,5},{1,4},{2,7},{3,6},{4,1},{5,0},{6,3},{7,2},{8,13},{9,12},{10,... | collective-permute-start | bytes 393224 | tf_op jit(solution)/shard_map/ppermute | solution.py:414
  90.1 12.4 %collective-permute-start.20 = (bf16[32,2176]{1,0:T(8,128)(2,1)S(1)}, bf16[32,2176]{1,0:T(8,128)(2,1)S(1)}, u32[]{:S(2)}, u32[]{:S(2)}) collective-permute-start(bf16[32,2176]{1,0:T(8,128)(2,1)S(1)} %get-tuple-element.127), channel_id=1, source_target_pairs={{0,2},{1,3},{2,0},{3,1},{4,6},{5,7},{6,4},{7,5},{8,10},{9,11},{10,... | collective-permute-start | bytes 417800 | tf_op jit(solution)/shard_map/ppermute | solution.py:414
  90.7 11.9 %collective-permute-start.21 = (bf16[32,2176]{1,0:T(8,128)(2,1)S(1)}, bf16[32,2176]{1,0:T(8,128)(2,1)S(1)}, u32[]{:S(2)}, u32[]{:S(2)}) collective-permute-start(bf16[32,2176]{1,0:T(8,128)(2,1)S(1)} %get-tuple-element.128), channel_id=1, source_target_pairs={{0,3},{1,2},{2,1},{3,0},{4,7},{5,6},{6,5},{7,4},{8,11},{9,10},{10,... | collective-permute-start | bytes 417800 | tf_op jit(solution)/shard_map/ppermute | solution.py:414
  103.8 11.6 %collective-permute-start.46 = (bf16[32,2176]{1,0:T(8,128)(2,1)S(1)}, bf16[32,2176]{1,0:T(8,128)(2,1)S(1)}, u32[]{:S(2)}, u32[]{:S(2)}) collective-permute-start(bf16[32,2176]{1,0:T(8,128)(2,1)S(1)} %get-tuple-element.162), channel_id=1, source_target_pairs={{0,3},{1,2},{2,1},{3,0},{4,7},{5,6},{6,5},{7,4},{8,11},{9,10},{10,... | collective-permute-start | bytes 417800 | tf_op jit(solution)/shard_map/ppermute | solution.py:414
  106.7 10.9 %collective-permute-start.47 = (bf16[32,2176]{1,0:T(8,128)(2,1)S(1)}, bf16[32,2176]{1,0:T(8,128)(2,1)S(1)}, u32[]{:S(2)}, u32[]{:S(2)}) collective-permute-start(bf16[32,2176]{1,0:T(8,128)(2,1)S(1)} %get-tuple-element.163), channel_id=1, source_target_pairs={{0,4},{1,5},{2,6},{3,7},{4,0},{5,1},{6,2},{7,3},{8,12},{9,13},{10,... | collective-permute-start | bytes 417800 | tf_op jit(solution)/shard_map/ppermute | solution.py:414
  115.4 18.4 %collective-permute-start.53 = (bf16[48,2176]{1,0:T(8,128)(2,1)S(1)}, bf16[48,2176]{1,0:T(8,128)(2,1)S(1)}, u32[]{:S(2)}, u32[]{:S(2)}) collective-permute-start(bf16[48,2176]{1,0:T(8,128)(2,1)S(1)} %get-tuple-element.169), channel_id=1, source_target_pairs={{0,8},{1,9},{2,10},{3,11},{4,12},{5,13},{6,14},{7,15},{8,16},{9,17... | collective-permute-start | bytes 626696 | tf_op jit(solution)/shard_map/ppermute | solution.py:418
  122.7 11.1 %collective-permute-start.51 = (bf16[48,2176]{1,0:T(8,128)(2,1)S(1)}, bf16[48,2176]{1,0:T(8,128)(2,1)S(1)}, u32[]{:S(2)}, u32[]{:S(2)}) collective-permute-start(bf16[48,2176]{1,0:T(8,128)(2,1)S(1)} %get-tuple-element.167), channel_id=1, source_target_pairs={{0,24},{1,25},{2,26},{3,27},{4,28},{5,29},{6,30},{7,31},{8,0},{9,1... | collective-permute-start | bytes 626696 | tf_op jit(solution)/shard_map/ppermute | solution.py:418
  123.4 17.1 %collective-permute-start.52 = (bf16[48,2176]{1,0:T(8,128)(2,1)S(1)}, bf16[48,2176]{1,0:T(8,128)(2,1)S(1)}, u32[]{:S(2)}, u32[]{:S(2)}) collective-permute-start(bf16[48,2176]{1,0:T(8,128)(2,1)S(1)} %get-tuple-element.168), channel_id=1, source_target_pairs={{0,16},{1,17},{2,18},{3,19},{4,20},{5,21},{6,22},{7,23},{8,24},{9,... | collective-permute-start | bytes 626696 | tf_op jit(solution)/shard_map/ppermute | solution.py:418
  (37 other events, 355.5 us)

commit v2 on v1

--- a/solution.py
+++ b/solution.py
@@ -12,6 +12,8 @@
 AXES = ("ep", "tp")
 GROUPS = 4
 META = 128
+LANES = 128
+LINES = 8
 GAIN_ROWS = 16
 FEATURE_TILES = 4
 SMALL_VMEM = 16 * 2**20
@@ -50,6 +52,31 @@
     return result
 
 
+def plane_shape(slots, features):
+    return (slots * (features // LANES) + LINES, LANES)
+
+
+def put_columns(ref, values, first, slots):
+    for tile in range(values.shape[1] // LANES):
+        row = (first // LANES + tile) * slots
+        ref[row : row + slots, :] = values[:, tile * LANES : (tile + 1) * LANES]
+
+
+def get_columns(target_ref, first, ref, slots):
+    for tile in range((ref.shape[0] - LINES) // slots):
+        block = ref[tile * slots : (tile + 1) * slots, :]
+        target_ref[first : first + slots, tile * LANES : (tile + 1) * LANES] = block
+
+
+def put_line(ref, lines, index, slots):
+    first = index * slots // LANES * LANES
+    ref[ref.shape[0] - LINES :, :] = lines[:LINES, first : first + LANES].astype(BF)
+
+
+def get_line(ref):
+    return ref[ref.shape[0] - LINES :, :].astype(F32)[0:1, :]
+
+
 def place(group_size):
     flat = lax.axis_index("ep") * lax.axis_size("tp") + lax.axis_index("tp")
     return lax.div(flat, group_size), lax.rem(flat, group_size)
@@ -60,7 +87,7 @@
     part_refs, refs = refs[6 : 6 + pieces], refs[6 + pieces :]
     out_refs, hot_ref = refs[:GROUPS], refs[GROUPS]
     tok_ref, routes_ref, gates_ref, gain_ref, lines_ref, sems = refs[GROUPS + 1 :]
-    rows, features = tok_ref.shape
+    rows, _ = tok_ref.shape
     width = moe_hbm.shape[1]
     me = lax.axis_index("tp")
     plane, _ = place(group_size)
@@ -107,12 +134,15 @@
         ),
         rows,
     ).astype(BF)
-    packed_meta = contract(hot, meta, 0, 0).astype(BF)
+    lines = []
+    for index in range(GROUPS):
+        slot = jnp.where(shift == index, rank, -1)
+        lines.append(contract(meta, one_hot(slot, LANES), 0, 0))
     copies[2].wait()
     packed = contract(hot, tok_ref[...], 0, 0).astype(BF)
-    for index in range(GROUPS):
-        out_refs[index][:, :features] = packed[index * share : (index + 1) * share]
-        out_refs[index][:, features:] = packed_meta[index * share : (index + 1) * share]
+    for index, ref in enumerate(out_refs):
+        put_columns(ref, packed[index * share : (index + 1) * share], 0, share)
+        put_line(ref, lines[index], 0, share)
 
     copies[3].wait()
     gain = gain_ref[...]
@@ -176,16 +206,14 @@
 def token_route_kernel(shifts, group_size, capacity, *refs):
     msg_refs, out_refs = refs[:shifts], refs[shifts : shifts + group_size]
     part_refs, full_ref = refs[shifts + group_size : -1], refs[-1]
-    share, width = msg_refs[0].shape
-    features = width - META
+    share = part_refs[0].shape[0]
     slots = shifts * capacity
     _, mine = place(group_size)
     lower = strict_lower(share)
     gates = []
     for index, ref in enumerate(msg_refs):
-        row = slice(index * share, (index + 1) * share)
-        full_ref[row, :] = ref[:, :features]
-        meta = ref[:, features:].astype(F32)
+        get_columns(full_ref, index * share, ref, share)
+        meta = ref[ref.shape[0] - LINES :, :].astype(F32).T[:share, :]
         gates.append((meta[:, 2:3], meta[:, 3:4]))
         experts = [meta[:, k : k + 1].astype(jnp.int32) - 1 for k in range(2)]
         members = [one_hot(e, META) for e in experts]
@@ -200,12 +228,11 @@
     total = shifts * share
     gate0 = lane_of((jnp.concatenate([g[0] for g in gates], axis=0),), total).astype(BF)
     gate1 = lane_of((jnp.concatenate([g[1] for g in gates], axis=0),), total).astype(BF)
-    packed_gate = contract(hot0, gate0, 0, 0) + contract(hot1, gate1, 0, 0)
+    lines = contract(gate0, hot0, 0, 0) + contract(gate1, hot1, 0, 0)
     packed = contract(hot0 + hot1, full_ref[...], 0, 0)
-    for index in range(group_size):
-        row = slice(index * slots, (index + 1) * slots)
-        out_refs[index][:, :features] = packed[row].astype(BF)
-        out_refs[index][:, features:] = packed_gate[row].astype(BF)
+    for index, ref in enumerate(out_refs):
+        put_columns(ref, packed[index * slots : (index + 1) * slots].astype(BF), 0, slots)
+        put_line(ref, lines, index, slots)
 
 
 def cot_route_kernel(shifts, group_size, capacity, *refs):
@@ -223,28 +250,39 @@
 
 def combine_kernel(shifts, group_size, capacity, *refs):
     piece_refs, part_refs = refs[:group_size], refs[group_size : group_size + shifts]
-    out_refs = refs[group_size + shifts :]
-    share, width = out_refs[0].shape
-    features = width - META
-    rows = jnp.concatenate([ref[...].astype(F32) for ref in piece_refs], axis=0).astype(BF)
+    out_refs, rows_ref = refs[group_size + shifts : -1], refs[-1]
+    share = part_refs[0].shape[0]
+    slots = shifts * capacity
+    lanes = lax.broadcasted_iota(jnp.int32, (1, LANES), 1)
+    lines = [jnp.zeros((1, LANES), F32) for _ in range(group_size * slots // LANES)]
+    for index, ref in enumerate(piece_refs):
+        get_columns(rows_ref, index * slots, ref, slots)
+        tile, first = divmod(index * slots, LANES)
+        mine = (lanes >= first) & (lanes < first + slots)
+        lines[tile] = jnp.where(mine, get_line(ref), lines[tile])
+    line = jnp.concatenate(lines, axis=1)
     hot0, hot1 = route_hots(part_refs, group_size, capacity)
-    summed = contract(hot0 + hot1, rows[:, :features], 1, 0).astype(BF)
-    grad0 = contract(hot0, rows[:, features:], 1, 0)[:, 0:1]
-    grad1 = contract(hot1, rows[:, features:], 1, 0)[:, 0:1]
-    meta = lane_of((grad0, grad1), shifts * share).astype(BF)
-    for index in range(shifts):
+    summed = contract(hot0 + hot1, rows_ref[...], 1, 0).astype(BF)
+    grad0 = jnp.sum(hot0.astype(F32) * line, axis=1, keepdims=True)
+    grad1 = jnp.sum(hot1.astype(F32) * line, axis=1, keepdims=True)
+    meta = lane_of((grad0, grad1), shifts * share)
+    empty = jnp.zeros((LANES - share, META), F32)
+    for index, ref in enumerate(out_refs):
         row = slice(index * share, (index + 1) * share)
-        out_refs[index][:, :features] = summed[row]
-        out_refs[index][:, features:] = meta[row]
+        put_columns(ref, summed[row], 0, share)
+        put_line(ref, jnp.concatenate([meta[row], empty], axis=0).T, 0, share)
 
 
 def finish_kernel(hot_ref, *refs):
-    msg_refs, tok_ref, gates_ref = refs[:GROUPS], refs[-2], refs[-1]
-    features = tok_ref.shape[1]
-    rows = jnp.concatenate([ref[...] for ref in msg_refs], axis=0)
+    msg_refs, tok_ref, gates_ref, rows_ref = refs[:GROUPS], *refs[-3:]
+    share = rows_ref.shape[0] // GROUPS
     hot = hot_ref[...]
-    tok_ref[...] = contract(hot, rows[:, :features], 1, 0).astype(BF)
-    grads = contract(rows[:, features:].astype(F32).T.astype(BF), hot, 1, 1)
+    grads = 0.0
+    for index, ref in enumerate(msg_refs):
+        get_columns(rows_ref, index * share, ref, share)
+        lines = ref[ref.shape[0] - LINES :, :share]
+        grads += contract(lines, hot[:, index * share : (index + 1) * share], 1, 1)
+    tok_ref[...] = contract(hot, rows_ref[...], 1, 0).astype(BF)
     gates_ref[...] = grads[0:2].astype(BF)
 
 
@@ -252,10 +290,15 @@
     count = len(refs) - 6
     piece_refs, (gate_ref, up_ref) = refs[:count], refs[count : count + 2]
     rows_ref, meta_ref, pre_gate_ref, pre_up_ref = refs[count + 2 :]
-    slots, features = piece_refs[0].shape[0], rows_ref.shape[1]
+    slots = rows_ref.shape[0] // count
+    line = lax.broadcasted_iota(jnp.int32, (slots, LANES), 0)
+    lane = lax.broadcasted_iota(jnp.int32, (slots, LANES), 1)
     for index, ref in enumerate(piece_refs):
-        rows_ref[index * slots : (index + 1) * slots, :] = ref[:, :features]
-        meta_ref[index * slots : (index + 1) * slots, :] = ref[:, features:]
+        get_columns(rows_ref, index * slots, ref, slots)
+        own = lane == line + index * slots % LANES
+        gate = jnp.sum(jnp.where(own, get_line(ref), 0.0), axis=1, keepdims=True)
+        gate = jnp.broadcast_to(gate, (slots, META)).astype(BF)
+        meta_ref[index * slots : (index + 1) * slots, :] = gate
     rows = rows_ref[...]
     pre_gate_ref[...] = contract(rows, gate_ref[0], 1, 0)
     pre_up_ref[...] = contract(rows, up_ref[0], 1, 0)
@@ -278,7 +321,7 @@
     sigmoid_gate = jax.nn.sigmoid(pre_gate)
     activated = pre_gate * sigmoid_gate
     hidden = activated * pre_up
-    grad = lane_of((jnp.sum(hidden * hid_grad, axis=1, keepdims=True),), rows).astype(BF)
+    lines = lane_of((jnp.sum(hidden * hid_grad, axis=1, keepdims=True),), rows).T
     d_hidden = weight * hid_grad
     d_gate_ref[...] = (
         d_hidden * pre_up * sigmoid_gate * (1.0 + pre_gate * (1.0 - sigmoid_gate))
@@ -291,9 +334,9 @@
         back = contract(d_gate_ref[...], gate_ref[0, column, :], 1, 1)
         back = (back + contract(d_up_ref[...], up_ref[0, column, :], 1, 1)).astype(BF)
         for index, ref in enumerate(out_refs):
-            ref[:, column] = back[index * slots : (index + 1) * slots]
+            put_columns(ref, back[index * slots : (index + 1) * slots], start, slots)
     for index, ref in enumerate(out_refs):
-        ref[:, features:] = grad[index * slots : (index + 1) * slots]
+        put_line(ref, lines, index, slots)
     scaled_ref[...] = (weight * cot_ref[...].astype(F32)).astype(BF)
 
 
@@ -322,7 +365,7 @@
 
 def forward_call(pieces, w_gate, w_up):
     features, hidden = w_gate.shape[1:]
-    rows = sum(p.shape[0] for p in pieces)
+    rows = sum((p.shape[0] - LINES) * LANES // features for p in pieces)
     return call(
         forward_kernel,
         [(rows, features), (rows, META), (rows, hidden, F32), (rows, hidden, F32)],
@@ -338,7 +381,7 @@
     rows = slots * len(pieces)
     result = call(
         functools.partial(backward_kernel, len(pieces)),
-        [(slots, features + META)] * len(pieces) + [(rows, hidden)] * 3 + [(rows, features)],
+        [plane_shape(slots, features)] * len(pieces) + [(rows, hidden)] * 3 + [(rows, features)],
         [*pieces, *held],
         scratch=[((rows, features), BF)],
         flops=6 * rows * features * hidden,
@@ -420,7 +463,7 @@
     part = [(tok_rows + GAIN_ROWS, 2 * moe_out.shape[1])] * pieces
     *out, hot = call(
         functools.partial(head_kernel, pieces, group_size, share),
-        part + [(share, wide)] * GROUPS + [(tok_rows, GROUPS * share)],
+        part + [plane_shape(share, features)] * GROUPS + [(tok_rows, GROUPS * share)],
         (tokens, routes.T, gates.T, moe_out, norm_gain[None, :], out_grad),
         scratch=[
             ((tok_rows, features), BF),
@@ -455,7 +498,7 @@
         slots = count * capacity
         out = call(
             functools.partial(token_route_kernel, count, group_size, capacity),
-            [(slots, wide)] * group_size + [(share, META)] * count,
+            [plane_shape(slots, features)] * group_size + [(share, META)] * count,
             [tok_at[s] for s in group],
             scratch=[((count * share, features), BF)],
             flops=2 * count * share * group_size * slots * wide,
@@ -488,8 +531,9 @@
         count = len(group)
         out = call(
             functools.partial(combine_kernel, count, group_size, capacity),
-            [(share, wide)] * count,
+            [plane_shape(share, features)] * count,
             [*back] + [parts[s] for s in group],
+            scratch=[((group_size * count * capacity, features), BF)],
             flops=2 * count * share * group_size * count * capacity * wide,
         )
         for s, array in zip(group, out):
@@ -498,6 +542,7 @@
         finish_kernel,
         [(tok_rows, features), (routes.shape[1], tok_rows)],
         [hot] + [home[s] for s in range(GROUPS)],
+        scratch=[((GROUPS * share, features), BF)],
         flops=2 * hot.size * wide,
     )
     return (token_grad, gates_grad.T, grad_gate, grad_up, grad_down)

time: 142 us -> 139 us (0.979)
  waiting for transfers between devices: 47 us -> 44.1 us
    ppermute x9, waiting for transfers between devices: 24.3 us -> 22.7 us  [over_z(): return lax.ppermute(array, AXES, pairs)]
  transfers between devices with their start and end apart: 54 -> 54, of which waited for: 17 -> 16; matrix products, arithmetic and copies ran while one was open for 0% -> 0% of each run, Pallas kernels for 16% -> 16%
where the time goes in v2:
time: 139 us
  starting transfers between devices  62.5 us (45%)
  waiting for transfers between devices  44.1 us (32%)
  Pallas kernels  26.9 us (19%)
  local copies, waits for them, and re-layouts  4.63 us (3%)
    ppermute x42, starting transfers between devices, over_plane(): return lax.ppermute(array, AXES, pairs)  41 us
    ppermute x9, waiting for transfers between devices, over_z(): return lax.ppermute(array, AXES, pairs)  22.7 us
    ppermute x42, waiting for transfers between devices, over_plane(): return lax.ppermute(array, AXES, pairs)  21.4 us
    ppermute x9, starting transfers between devices, over_z(): return lax.ppermute(array, AXES, pairs)  19.9 us
    pallas_call x13, Pallas kernels, call(): pl.pallas_call(kernel, out_shape=outs, in_specs=[pl.BlockSpec(memory_spac...  19.5 us
    pallas_call x1, Pallas kernels, weight_call(): pl.pallas_call(functools.partial(weight_kernel, len(kept)), grid=(FEATURE...  7.42 us
    unnamed x14, local copies, waits for them, and re-layouts  4.63 us
  transfers between devices with their start and end apart: 54, of which 16 were waited for; matrix products, arithmetic and copies ran while one was open for 0% of the time, Pallas kernels for 16%

profile of v2, /device:TPU:0, one launch (start us, length us, event | category | flops | bytes accessed | tf_op | source)
XLA Modules:
  0.0 139.0 jit_solution(8184484229855284687)
XLA Ops:
  0.6 3.4 %shard_map.128 = (bf16[144,1024]{1,0:T(8,128)(2,1)}, bf16[144,1024]{1,0:T(8,128)(2,1)}, bf16[144,1024]{1,0:T(8,128)(2,1)}, bf16[144,1024]{1,0:T(8,128)(2,1)}, bf...) custom-call(bf16[128,2048]{1,0:T(8,128)(2,1)} %refs_0_.1, ...), custom_call_target="tpu_custom_call" | custom-call | flops 106954752 | bytes 3600384 | tf_op jit(solution)/shard_map/pallas_call | solution.py:428
  4.0 3.1 %collective-permute-start.28 = (bf16[776,128]{1,0:T(8,128)(2,1)}, bf16[776,128]{1,0:T(8,128)(2,1)S(1)}, u32[]{:S(2)}, u32[]{:S(2)}) collective-permute-start(bf16[776,128]{1,0:T(8,128)(2,1)} %get-tuple-element.136), channel_id=1, source_target_pairs={{0,8},{1,9},{2,10},{3,11},{4,12},{5,13},{6,14},{7,15},{8,16},{9,17... | collective-permute-start | bytes 595976 | tf_op jit(solution)/shard_map/ppermute | solution.py:461
  8.7 2.6 %collective-permute-start.29 = (bf16[776,128]{1,0:T(8,128)(2,1)}, bf16[776,128]{1,0:T(8,128)(2,1)S(1)}, u32[]{:S(2)}, u32[]{:S(2)}) collective-permute-start(bf16[776,128]{1,0:T(8,128)(2,1)} %get-tuple-element.137), channel_id=1, source_target_pairs={{0,16},{1,17},{2,18},{3,19},{4,20},{5,21},{6,22},{7,23},{8,24},{9,... | collective-permute-start | bytes 595976 | tf_op jit(solution)/shard_map/ppermute | solution.py:461
  11.3 3.8 %collective-permute-done.28.refs_0_ = bf16[776,128]{1,0:T(8,128)(2,1)S(1)} collective-permute-done((bf16[776,128]{1,0:T(8,128)(2,1)}, bf16[776,128]{1,0:T(8,128)(2,1)S(1)}, u32[]{:S(2)}, u32[]{:S(2)}) %collective-permute-start.28) | collective-permute-done | bytes 198688 | tf_op jit(solution)/shard_map/ppermute | solution.py:461
  16.7 6.2 %collective-permute-done.29.refs_1_ = bf16[776,128]{1,0:T(8,128)(2,1)S(1)} collective-permute-done((bf16[776,128]{1,0:T(8,128)(2,1)}, bf16[776,128]{1,0:T(8,128)(2,1)S(1)}, u32[]{:S(2)}, u32[]{:S(2)}) %collective-permute-start.29) | collective-permute-done | bytes 198688 | tf_op jit(solution)/shard_map/ppermute | solution.py:461
  24.0 2.7 %collective-permute-done.4.refs_0_ = bf16[776,128]{1,0:T(8,128)(2,1)S(1)} collective-permute-done((bf16[776,128]{1,0:T(8,128)(2,1)}, bf16[776,128]{1,0:T(8,128)(2,1)S(1)}, u32[]{:S(2)}, u32[]{:S(2)}) %collective-permute-start.4) | collective-permute-done | bytes 198688 | tf_op jit(solution)/shard_map/ppermute | solution.py:461
  30.2 2.5 %collective-permute-start.42 = (bf16[520,128]{1,0:T(8,128)(2,1)S(1)}, bf16[520,128]{1,0:T(8,128)(2,1)S(1)}, u32[]{:S(2)}, u32[]{:S(2)}) collective-permute-start(bf16[520,128]{1,0:T(8,128)(2,1)S(1)} %get-tuple-element.154), channel_id=1, source_target_pairs={{0,6},{1,7},{2,4},{3,5},{4,2},{5,3},{6,0},{7,1},{8,14},{9,15},{10,... | collective-permute-start | bytes 399368 | tf_op jit(solution)/shard_map/ppermute | solution.py:457
  35.4 3.2 %collective-permute-start.3 = (bf16[48,2048]{1,0:T(8,128)(2,1)S(1)}, bf16[48,2048]{1,0:T(8,128)(2,1)S(1)}, u32[]{:S(2)}, u32[]{:S(2)}) collective-permute-start(bf16[48,2048]{1,0:T(8,128)(2,1)S(1)} %get-tuple-element.100), channel_id=1, source_target_pairs={{0,24},{1,25},{2,26},{3,27},{4,28},{5,29},{6,30},{7,31},{8,0},{9,1... | collective-permute-start | bytes 589832 | tf_op jit(solution)/shard_map/ppermute | solution.py:461
  38.6 2.7 %collective-permute-start.27 = (bf16[48,2048]{1,0:T(8,128)(2,1)S(1)}, bf16[48,2048]{1,0:T(8,128)(2,1)S(1)}, u32[]{:S(2)}, u32[]{:S(2)}) collective-permute-start(bf16[48,2048]{1,0:T(8,128)(2,1)S(1)} %get-tuple-element.135), channel_id=1, source_target_pairs={{0,16},{1,17},{2,18},{3,19},{4,20},{5,21},{6,22},{7,23},{8,24},{9,... | collective-permute-start | bytes 589832 | tf_op jit(solution)/shard_map/ppermute | solution.py:461
  45.2 4.6 %collective-permute-done.13.refs_2_ = bf16[520,128]{1,0:T(8,128)(2,1)S(1)} collective-permute-done((bf16[520,128]{1,0:T(8,128)(2,1)S(1)}, bf16[520,128]{1,0:T(8,128)(2,1)S(1)}, u32[]{:S(2)}, u32[]{:S(2)}) %collective-permute-start.13) | collective-permute-done | bytes 133152 | tf_op jit(solution)/shard_map/ppermute | solution.py:457
  51.9 4.0 %collective-permute-done.27.refs_1_ = bf16[48,2048]{1,0:T(8,128)(2,1)S(1)} collective-permute-done((bf16[48,2048]{1,0:T(8,128)(2,1)S(1)}, bf16[48,2048]{1,0:T(8,128)(2,1)S(1)}, u32[]{:S(2)}, u32[]{:S(2)}) %collective-permute-start.27) | collective-permute-done | bytes 196640 | tf_op jit(solution)/shard_map/ppermute | solution.py:461
  57.7 2.2 %collective-permute-start.43 = (bf16[520,128]{1,0:T(8,128)(2,1)S(1)}, bf16[520,128]{1,0:T(8,128)(2,1)S(1)}, u32[]{:S(2)}, u32[]{:S(2)}) collective-permute-start(bf16[520,128]{1,0:T(8,128)(2,1)S(1)} %get-tuple-element.155), channel_id=1, source_target_pairs={{0,7},{1,6},{2,5},{3,4},{4,3},{5,2},{6,1},{7,0},{8,15},{9,14},{10,... | collective-permute-start | bytes 399368 | tf_op jit(solution)/shard_map/ppermute | solution.py:457
  78.5 3.7 %collective-permute-done.10.refs_6_ = bf16[32,2048]{1,0:T(8,128)(2,1)S(1)} collective-permute-done((bf16[32,2048]{1,0:T(8,128)(2,1)S(1)}, bf16[32,2048]{1,0:T(8,128)(2,1)S(1)}, u32[]{:S(2)}, u32[]{:S(2)}) %collective-permute-start.10) | collective-permute-done | bytes 131104 | tf_op jit(solution)/shard_map/ppermute | solution.py:457
  82.4 2.2 %collective-permute-start.36 = (bf16[32,2048]{1,0:T(8,128)(2,1)S(1)}, bf16[32,2048]{1,0:T(8,128)(2,1)S(1)}, u32[]{:S(2)}, u32[]{:S(2)}) collective-permute-start(bf16[32,2048]{1,0:T(8,128)(2,1)S(1)} %get-tuple-element.147), channel_id=1, source_target_pairs={{0,7},{1,6},{2,5},{3,4},{4,3},{5,2},{6,1},{7,0},{8,15},{9,14},{10,... | collective-permute-start | bytes 393224 | tf_op jit(solution)/shard_map/ppermute | solution.py:457
  84.6 3.1 %shard_map.133 = (bf16[520,128]{1,0:T(8,128)(2,1)S(1)}, bf16[520,128]{1,0:T(8,128)(2,1)S(1)}, bf16[520,128]{1,0:T(8,128)(2,1)S(1)}, bf16[520,128]{1,0:T(8,128)(2...) custom-call(bf16[32,2048]{1,0:T(8,128)(2,1)S(1)} %get-tuple-element., ...), custom_call_target="tpu_custom_call" | custom-call | flops 2415919104 | bytes 15417344 | tf_op jit(solution)/shard_map/pallas_call | solution.py:428
  90.9 2.5 %collective-permute-done.35.refs_6_ = bf16[32,2048]{1,0:T(8,128)(2,1)S(1)} collective-permute-done((bf16[32,2048]{1,0:T(8,128)(2,1)S(1)}, bf16[32,2048]{1,0:T(8,128)(2,1)S(1)}, u32[]{:S(2)}, u32[]{:S(2)}) %collective-permute-start.35) | collective-permute-done | bytes 131104 | tf_op jit(solution)/shard_map/ppermute | solution.py:457
  94.9 3.0 %shard_map.138 = (bf16[520,128]{1,0:T(8,128)(2,1)S(1)}, bf16[520,128]{1,0:T(8,128)(2,1)S(1)}, bf16[520,128]{1,0:T(8,128)(2,1)S(1)}, bf16[520,128]{1,0:T(8,128)(2...) custom-call(bf16[32,2048]{1,0:T(8,128)(2,1)S(1)} %get-tuple-element., ...), custom_call_target="tpu_custom_call" | custom-call | flops 2415919104 | bytes 15417344 | tf_op jit(solution)/shard_map/pallas_call | solution.py:428
  98.0 2.8 %collective-permute-start.24 = (bf16[520,128]{1,0:T(8,128)(2,1)S(1)}, bf16[520,128]{1,0:T(8,128)(2,1)S(1)}, u32[]{:S(2)}, u32[]{:S(2)}) collective-permute-start(bf16[520,128]{1,0:T(8,128)(2,1)S(1)} %get-tuple-element.131), channel_id=1, source_target_pairs={{0,6},{1,7},{2,4},{3,5},{4,2},{5,3},{6,0},{7,1},{8,14},{9,15},{10,... | collective-permute-start | bytes 399368 | tf_op jit(solution)/shard_map/ppermute | solution.py:457
  102.8 2.7 %collective-permute-done.24.refs_6_ = bf16[520,128]{1,0:T(8,128)(2,1)S(1)} collective-permute-done((bf16[520,128]{1,0:T(8,128)(2,1)S(1)}, bf16[520,128]{1,0:T(8,128)(2,1)S(1)}, u32[]{:S(2)}, u32[]{:S(2)}) %collective-permute-start.24) | collective-permute-done | bytes 133152 | tf_op jit(solution)/shard_map/ppermute | solution.py:457
  113.5 2.1 %collective-permute-start.53 = (bf16[776,128]{1,0:T(8,128)(2,1)S(1)}, bf16[776,128]{1,0:T(8,128)(2,1)S(1)}, u32[]{:S(2)}, u32[]{:S(2)}) collective-permute-start(bf16[776,128]{1,0:T(8,128)(2,1)S(1)} %get-tuple-element.169), channel_id=1, source_target_pairs={{0,8},{1,9},{2,10},{3,11},{4,12},{5,13},{6,14},{7,15},{8,16},{9,17... | collective-permute-start | bytes 595976 | tf_op jit(solution)/shard_map/ppermute | solution.py:461
  117.2 2.0 %collective-permute-done.50.refs_7_ = bf16[520,128]{1,0:T(8,128)(2,1)S(1)} collective-permute-done((bf16[520,128]{1,0:T(8,128)(2,1)S(1)}, bf16[520,128]{1,0:T(8,128)(2,1)S(1)}, u32[]{:S(2)}, u32[]{:S(2)}) %collective-permute-start.50) | collective-permute-done | bytes 133152 | tf_op jit(solution)/shard_map/ppermute | solution.py:457
  119.7 2.7 %collective-permute-start.51 = (bf16[776,128]{1,0:T(8,128)(2,1)S(1)}, bf16[776,128]{1,0:T(8,128)(2,1)S(1)}, u32[]{:S(2)}, u32[]{:S(2)}) collective-permute-start(bf16[776,128]{1,0:T(8,128)(2,1)S(1)} %get-tuple-element.167), channel_id=1, source_target_pairs={{0,24},{1,25},{2,26},{3,27},{4,28},{5,29},{6,30},{7,31},{8,0},{9,1... | collective-permute-start | bytes 595976 | tf_op jit(solution)/shard_map/ppermute | solution.py:461
  124.3 7.4 %shard_map.141 = (bf16[1,2048,768]{2,1,0:T(8,128)(2,1)}, bf16[1,2048,768]{2,1,0:T(8,128)(2,1)}, bf16[1,768,2048]{2,1,0:T(8,128)(2,1)}) custom-call(bf16[256,2048]{1,0:T(8,128)(2,1)S(1)} %get-tuple-element.172.refs_0_, bf16[256,2048]{1,0:T(8,128)(2,1)S(1)} %get-tuple-element.173.refs_1_, bf16[256,768]{1,0:T(8,128)(2,1)S(1)} %get-tuple-element.174.refs_2_, ...), custom_call_target="tpu_custom_call" | custom-call | flops 4831838208 | bytes 15990784 | tf_op jit(solution)/shard_map/pallas_call | solution.py:399
  131.7 6.0 %collective-permute-done.52.refs_2_ = bf16[776,128]{1,0:T(8,128)(2,1)S(1)} collective-permute-done((bf16[776,128]{1,0:T(8,128)(2,1)S(1)}, bf16[776,128]{1,0:T(8,128)(2,1)S(1)}, u32[]{:S(2)}, u32[]{:S(2)}) %collective-permute-start.52) | collective-permute-done | bytes 198688 | tf_op jit(solution)/shard_map/ppermute | solution.py:461
  (112 shorter events, 57.0 us)
Async XLA Ops:
  4.0 11.1 %collective-permute-start.28 = (bf16[776,128]{1,0:T(8,128)(2,1)}, bf16[776,128]{1,0:T(8,128)(2,1)S(1)}, u32[]{:S(2)}, u32[]{:S(2)}) collective-permute-start(bf16[776,128]{1,0:T(8,128)(2,1)} %get-tuple-element.136), channel_id=1, source_target_pairs={{0,8},{1,9},{2,10},{3,11},{4,12},{5,13},{6,14},{7,15},{8,16},{9,17... | collective-permute-start | bytes 595976 | tf_op jit(solution)/shard_map/ppermute | solution.py:461
  7.1 21.1 %collective-permute-start = (bf16[144,1024]{1,0:T(8,128)(2,1)}, bf16[144,1024]{1,0:T(8,128)(2,1)S(1)}, u32[]{:S(2)}, u32[]{:S(2)}) collective-permute-start(bf16[144,1024]{1,0:T(8,128)(2,1)} %get-tuple-element.97), channel_id=1, source_target_pairs={{0,1},{1,0},{2,3},{3,2},{4,5},{5,4},{6,7},{7,6},{8,9},{9,8},{10,11... | collective-permute-start | bytes 884744 | tf_op jit(solution)/shard_map/ppermute | solution.py:451
  7.2 21.2 %collective-permute-start.1 = (bf16[144,1024]{1,0:T(8,128)(2,1)}, bf16[144,1024]{1,0:T(8,128)(2,1)S(1)}, u32[]{:S(2)}, u32[]{:S(2)}) collective-permute-start(bf16[144,1024]{1,0:T(8,128)(2,1)} %get-tuple-element.98), channel_id=1, source_target_pairs={{0,2},{1,3},{2,0},{3,1},{4,6},{5,7},{6,4},{7,5},{8,10},{9,11},{10,... | collective-permute-start | bytes 884744 | tf_op jit(solution)/shard_map/ppermute | solution.py:451
  8.7 14.2 %collective-permute-start.29 = (bf16[776,128]{1,0:T(8,128)(2,1)}, bf16[776,128]{1,0:T(8,128)(2,1)S(1)}, u32[]{:S(2)}, u32[]{:S(2)}) collective-permute-start(bf16[776,128]{1,0:T(8,128)(2,1)} %get-tuple-element.137), channel_id=1, source_target_pairs={{0,16},{1,17},{2,18},{3,19},{4,20},{5,21},{6,22},{7,23},{8,24},{9,... | collective-permute-start | bytes 595976 | tf_op jit(solution)/shard_map/ppermute | solution.py:461
  11.3 18.6 %collective-permute-start.2 = (bf16[144,1024]{1,0:T(8,128)(2,1)}, bf16[144,1024]{1,0:T(8,128)(2,1)S(1)}, u32[]{:S(2)}, u32[]{:S(2)}) collective-permute-start(bf16[144,1024]{1,0:T(8,128)(2,1)} %get-tuple-element.99), channel_id=1, source_target_pairs={{0,3},{1,2},{2,1},{3,0},{4,7},{5,6},{6,5},{7,4},{8,11},{9,10},{10,... | collective-permute-start | bytes 884744 | tf_op jit(solution)/shard_map/ppermute | solution.py:451
  15.1 11.6 %collective-permute-start.4 = (bf16[776,128]{1,0:T(8,128)(2,1)}, bf16[776,128]{1,0:T(8,128)(2,1)S(1)}, u32[]{:S(2)}, u32[]{:S(2)}) collective-permute-start(bf16[776,128]{1,0:T(8,128)(2,1)} %get-tuple-element.102), channel_id=1, source_target_pairs={{0,24},{1,25},{2,26},{3,27},{4,28},{5,29},{6,30},{7,31},{8,0},{9,1... | collective-permute-start | bytes 595976 | tf_op jit(solution)/shard_map/ppermute | solution.py:461
  29.9 13.4 %collective-permute-start.41 = (bf16[520,128]{1,0:T(8,128)(2,1)S(1)}, bf16[520,128]{1,0:T(8,128)(2,1)S(1)}, u32[]{:S(2)}, u32[]{:S(2)}) collective-permute-start(bf16[520,128]{1,0:T(8,128)(2,1)S(1)} %get-tuple-element.153), channel_id=1, source_target_pairs={{0,5},{1,4},{2,7},{3,6},{4,1},{5,0},{6,3},{7,2},{8,13},{9,12},{10,... | collective-permute-start | bytes 399368 | tf_op jit(solution)/shard_map/ppermute | solution.py:457
  30.2 13.2 %collective-permute-start.42 = (bf16[520,128]{1,0:T(8,128)(2,1)S(1)}, bf16[520,128]{1,0:T(8,128)(2,1)S(1)}, u32[]{:S(2)}, u32[]{:S(2)}) collective-permute-start(bf16[520,128]{1,0:T(8,128)(2,1)S(1)} %get-tuple-element.154), channel_id=1, source_target_pairs={{0,6},{1,7},{2,4},{3,5},{4,2},{5,3},{6,0},{7,1},{8,14},{9,15},{10,... | collective-permute-start | bytes 399368 | tf_op jit(solution)/shard_map/ppermute | solution.py:457
  35.4 15.0 %collective-permute-start.3 = (bf16[48,2048]{1,0:T(8,128)(2,1)S(1)}, bf16[48,2048]{1,0:T(8,128)(2,1)S(1)}, u32[]{:S(2)}, u32[]{:S(2)}) collective-permute-start(bf16[48,2048]{1,0:T(8,128)(2,1)S(1)} %get-tuple-element.100), channel_id=1, source_target_pairs={{0,24},{1,25},{2,26},{3,27},{4,28},{5,29},{6,30},{7,31},{8,0},{9,1... | collective-permute-start | bytes 589832 | tf_op jit(solution)/shard_map/ppermute | solution.py:461
  38.6 11.8 %collective-permute-start.26 = (bf16[48,2048]{1,0:T(8,128)(2,1)S(1)}, bf16[48,2048]{1,0:T(8,128)(2,1)S(1)}, u32[]{:S(2)}, u32[]{:S(2)}) collective-permute-start(bf16[48,2048]{1,0:T(8,128)(2,1)S(1)} %get-tuple-element.134), channel_id=1, source_target_pairs={{0,8},{1,9},{2,10},{3,11},{4,12},{5,13},{6,14},{7,15},{8,16},{9,17... | collective-permute-start | bytes 589832 | tf_op jit(solution)/shard_map/ppermute | solution.py:461
  38.6 17.3 %collective-permute-start.27 = (bf16[48,2048]{1,0:T(8,128)(2,1)S(1)}, bf16[48,2048]{1,0:T(8,128)(2,1)S(1)}, u32[]{:S(2)}, u32[]{:S(2)}) collective-permute-start(bf16[48,2048]{1,0:T(8,128)(2,1)S(1)} %get-tuple-element.135), channel_id=1, source_target_pairs={{0,16},{1,17},{2,18},{3,19},{4,20},{5,21},{6,22},{7,23},{8,24},{9,... | collective-permute-start | bytes 589832 | tf_op jit(solution)/shard_map/ppermute | solution.py:461
  44.7 13.0 %collective-permute-start.14 = (bf16[520,128]{1,0:T(8,128)(2,1)S(1)}, bf16[520,128]{1,0:T(8,128)(2,1)S(1)}, u32[]{:S(2)}, u32[]{:S(2)}) collective-permute-start(bf16[520,128]{1,0:T(8,128)(2,1)S(1)} %get-tuple-element.117), channel_id=1, source_target_pairs={{0,3},{1,2},{2,1},{3,0},{4,7},{5,6},{6,5},{7,4},{8,11},{9,10},{10,... | collective-permute-start | bytes 399368 | tf_op jit(solution)/shard_map/ppermute | solution.py:457
  50.4 11.1 %collective-permute-start.17 = (bf16[520,128]{1,0:T(8,128)(2,1)S(1)}, bf16[520,128]{1,0:T(8,128)(2,1)S(1)}, u32[]{:S(2)}, u32[]{:S(2)}) collective-permute-start(bf16[520,128]{1,0:T(8,128)(2,1)S(1)} %get-tuple-element.120), channel_id=1, source_target_pairs={{0,6},{1,7},{2,4},{3,5},{4,2},{5,3},{6,0},{7,1},{8,14},{9,15},{10,... | collective-permute-start | bytes 399368 | tf_op jit(solution)/shard_map/ppermute | solution.py:457
  70.5 11.7 %collective-permute-start.10 = (bf16[32,2048]{1,0:T(8,128)(2,1)S(1)}, bf16[32,2048]{1,0:T(8,128)(2,1)S(1)}, u32[]{:S(2)}, u32[]{:S(2)}) collective-permute-start(bf16[32,2048]{1,0:T(8,128)(2,1)S(1)} %get-tuple-element.112), channel_id=1, source_target_pairs={{0,6},{1,7},{2,4},{3,5},{4,2},{5,3},{6,0},{7,1},{8,14},{9,15},{10,... | collective-permute-start | bytes 393224 | tf_op jit(solution)/shard_map/ppermute | solution.py:457
  75.4 12.3 %collective-permute-start.32 = (bf16[32,2048]{1,0:T(8,128)(2,1)S(1)}, bf16[32,2048]{1,0:T(8,128)(2,1)S(1)}, u32[]{:S(2)}, u32[]{:S(2)}) collective-permute-start(bf16[32,2048]{1,0:T(8,128)(2,1)S(1)} %get-tuple-element.143), channel_id=1, source_target_pairs={{0,3},{1,2},{2,1},{3,0},{4,7},{5,6},{6,5},{7,4},{8,11},{9,10},{10,... | collective-permute-start | bytes 393224 | tf_op jit(solution)/shard_map/ppermute | solution.py:457
  76.0 12.4 %collective-permute-start.33 = (bf16[32,2048]{1,0:T(8,128)(2,1)S(1)}, bf16[32,2048]{1,0:T(8,128)(2,1)S(1)}, u32[]{:S(2)}, u32[]{:S(2)}) collective-permute-start(bf16[32,2048]{1,0:T(8,128)(2,1)S(1)} %get-tuple-element.144), channel_id=1, source_target_pairs={{0,4},{1,5},{2,6},{3,7},{4,0},{5,1},{6,2},{7,3},{8,12},{9,13},{10,... | collective-permute-start | bytes 393224 | tf_op jit(solution)/shard_map/ppermute | solution.py:457
  77.4 11.6 %collective-permute-start.34 = (bf16[32,2048]{1,0:T(8,128)(2,1)S(1)}, bf16[32,2048]{1,0:T(8,128)(2,1)S(1)}, u32[]{:S(2)}, u32[]{:S(2)}) collective-permute-start(bf16[32,2048]{1,0:T(8,128)(2,1)S(1)} %get-tuple-element.145), channel_id=1, source_target_pairs={{0,5},{1,4},{2,7},{3,6},{4,1},{5,0},{6,3},{7,2},{8,13},{9,12},{10,... | collective-permute-start | bytes 393224 | tf_op jit(solution)/shard_map/ppermute | solution.py:457
  82.2 11.2 %collective-permute-start.35 = (bf16[32,2048]{1,0:T(8,128)(2,1)S(1)}, bf16[32,2048]{1,0:T(8,128)(2,1)S(1)}, u32[]{:S(2)}, u32[]{:S(2)}) collective-permute-start(bf16[32,2048]{1,0:T(8,128)(2,1)S(1)} %get-tuple-element.146), channel_id=1, source_target_pairs={{0,6},{1,7},{2,4},{3,5},{4,2},{5,3},{6,0},{7,1},{8,14},{9,15},{10,... | collective-permute-start | bytes 393224 | tf_op jit(solution)/shard_map/ppermute | solution.py:457
  88.4 12.4 %collective-permute-start.20 = (bf16[520,128]{1,0:T(8,128)(2,1)S(1)}, bf16[520,128]{1,0:T(8,128)(2,1)S(1)}, u32[]{:S(2)}, u32[]{:S(2)}) collective-permute-start(bf16[520,128]{1,0:T(8,128)(2,1)S(1)} %get-tuple-element.127), channel_id=1, source_target_pairs={{0,2},{1,3},{2,0},{3,1},{4,6},{5,7},{6,4},{7,5},{8,10},{9,11},{10,... | collective-permute-start | bytes 399368 | tf_op jit(solution)/shard_map/ppermute | solution.py:457
  88.9 12.0 %collective-permute-start.21 = (bf16[520,128]{1,0:T(8,128)(2,1)S(1)}, bf16[520,128]{1,0:T(8,128)(2,1)S(1)}, u32[]{:S(2)}, u32[]{:S(2)}) collective-permute-start(bf16[520,128]{1,0:T(8,128)(2,1)S(1)} %get-tuple-element.128), channel_id=1, source_target_pairs={{0,3},{1,2},{2,1},{3,0},{4,7},{5,6},{6,5},{7,4},{8,11},{9,10},{10,... | collective-permute-start | bytes 399368 | tf_op jit(solution)/shard_map/ppermute | solution.py:457
  102.2 11.4 %collective-permute-start.46 = (bf16[520,128]{1,0:T(8,128)(2,1)S(1)}, bf16[520,128]{1,0:T(8,128)(2,1)S(1)}, u32[]{:S(2)}, u32[]{:S(2)}) collective-permute-start(bf16[520,128]{1,0:T(8,128)(2,1)S(1)} %get-tuple-element.162), channel_id=1, source_target_pairs={{0,3},{1,2},{2,1},{3,0},{4,7},{5,6},{6,5},{7,4},{8,11},{9,10},{10,... | collective-permute-start | bytes 399368 | tf_op jit(solution)/shard_map/ppermute | solution.py:457
  113.5 18.2 %collective-permute-start.53 = (bf16[776,128]{1,0:T(8,128)(2,1)S(1)}, bf16[776,128]{1,0:T(8,128)(2,1)S(1)}, u32[]{:S(2)}, u32[]{:S(2)}) collective-permute-start(bf16[776,128]{1,0:T(8,128)(2,1)S(1)} %get-tuple-element.169), channel_id=1, source_target_pairs={{0,8},{1,9},{2,10},{3,11},{4,12},{5,13},{6,14},{7,15},{8,16},{9,17... | collective-permute-start | bytes 595976 | tf_op jit(solution)/shard_map/ppermute | solution.py:461
  119.7 12.0 %collective-permute-start.51 = (bf16[776,128]{1,0:T(8,128)(2,1)S(1)}, bf16[776,128]{1,0:T(8,128)(2,1)S(1)}, u32[]{:S(2)}, u32[]{:S(2)}) collective-permute-start(bf16[776,128]{1,0:T(8,128)(2,1)S(1)} %get-tuple-element.167), channel_id=1, source_target_pairs={{0,24},{1,25},{2,26},{3,27},{4,28},{5,29},{6,30},{7,31},{8,0},{9,1... | collective-permute-start | bytes 595976 | tf_op jit(solution)/shard_map/ppermute | solution.py:461
  122.4 15.3 %collective-permute-start.52 = (bf16[776,128]{1,0:T(8,128)(2,1)S(1)}, bf16[776,128]{1,0:T(8,128)(2,1)S(1)}, u32[]{:S(2)}, u32[]{:S(2)}) collective-permute-start(bf16[776,128]{1,0:T(8,128)(2,1)S(1)} %get-tuple-element.168), channel_id=1, source_target_pairs={{0,16},{1,17},{2,18},{3,19},{4,20},{5,21},{6,22},{7,23},{8,24},{9,... | collective-permute-start | bytes 595976 | tf_op jit(solution)/shard_map/ppermute | solution.py:461
  (37 other events, 347.1 us)
